TPU v7x, 512 devices: a 4x2x32 block of a 4x8x32 slice. The times are simulated.
512 devices in a mesh: grp: 2 (over y), kv: 64 (over z, core), tp: 4 (over x).
Axes of the slice: x: 4, y: 2, z: 32, core: 2. Of those that a mesh axis runs over, the one named last changes fastest.
The devices are a block of a 4x8x32 slice.
Arguments:
- piece_rows: bfloat16 [8192, 2048], P(('grp', 'kv')), parts along dimension 0, may hold values from -6 to 6
- dec_rows: bfloat16 [256, 2048], P(('grp', 'kv')), parts along dimension 0, may hold values from -6 to 6
- norm_gain: float32 [2048], replicated, may hold values from 0.1 to 1.9
- w_query: bfloat16 [2048, 1024], P(None, 'tp'), may hold values from -0.25 to 0.25
- w_key: bfloat16 [2048, 256], P(None, 'tp'), may hold values from -0.125 to 0.125
- w_value: bfloat16 [2048, 256], P(None, 'tp'), may hold values from -0.125 to 0.125
- w_forget: bfloat16 [2048, 16], P(None, 'tp'), may hold values from -0.125 to 0.125
- forget_bias: float32 [16], P('tp'), may hold values from 3 to 12
- piece_decay: float32 [16, 8192], P('tp', ('grp', 'kv')), parts along dimension 1, may hold values from -3 to 0
- cache_kv: bfloat16 [98304, 4, 128], P(('grp', 'kv'), 'tp'), parts along dimension 0, may hold values from -150 to 150
- cache_gate: float32 [16, 98304], P('tp', ('grp', 'kv')), parts along dimension 1, may hold values from -2460.6 to 0, as said below
- dec_cache: bfloat16 [256, 3072, 4, 128], P(('grp', 'kv'), None, 'tp'), parts along dimension 0, may hold values from -150 to 150
- dec_gate: float32 [256, 16, 3072], P(('grp', 'kv'), 'tp'), parts along dimension 0, may hold values from -156.6 to 0, as said below
- dec_lengths: int32 [256], P(('grp', 'kv')), parts along dimension 0, may hold values from 1 to 3072, as said below
- w_out: bfloat16 [1024, 2048], P(None, 'tp'), may hold values from -0.75 to 0.75
Outputs:
- piece_out: bfloat16 [8192, 2048], P(('grp', 'kv'), 'tp'), parts along dimension 0
- dec_out: bfloat16 [256, 2048], P(('grp', 'kv'), 'tp'), parts along dimension 0
There are 2 independent parts, one for each index of `grp`. A program takes and returns all parts, laid end to end along the dimension named above; an argument that names none is the same for every part. Nothing has to cross between parts.
Inputs may be any that keep to these rules, and one draw needn't show every extreme that they name: `cache_gate`: each head's values never fall from one position to the next and are 0 at the last cached position. `dec_gate`: each sequence's and head's values never rise from one position to the next. Sequence b's cache holds its first dec_lengths[b] positions; in each part some sequence holds 3072.
All inputs are finite; a program needn't handle non-finite values.
Results may differ from a plain program's by a relative error of at most 0.006.
The roundings to bfloat16 on the way count: a program that leaves them out, or rounds other values in their place, can miss the bound.
Values may be sent and summed in bfloat16 or wider, within the bound.
No kernel may reach another device: no remote copies, remote signals or barrier semaphores. Data moves between devices by JAX's collectives and lax.ppermute only.
A program may use at most 64 MiB of HBM per device.

v0:
```python
import jax
import jax.numpy as jnp
from jax import lax
from jax.sharding import Mesh
from jax.sharding import PartitionSpec as P

KV = ("kv_0", "kv_1")
GRP_KV = ("grp", "kv_0", "kv_1")


def carried_in(array, axis, combine, identity):
    length, mine = (lax.axis_size(axis), lax.axis_index(axis))
    everything = lax.all_gather(array, axis)
    start = jnp.broadcast_to(jnp.asarray(identity, array.dtype), array.shape)

    def lap(k, before):
        reached = k < mine
        new = combine(before, everything[k])
        return jnp.where(reached, new, before)

    return lax.fori_loop(0, length, lap, start)


def in_order(blocks, dim):
    blocks = jnp.moveaxis(blocks, 0, dim)
    lengths = blocks.shape
    return blocks.reshape(*lengths[:dim], lengths[dim] * lengths[dim + 1], *lengths[dim + 2 :])


def stacked_from(array, axes, turns):
    blocks = array
    for k in turns:
        blocks = lax.all_gather(blocks, axes[k])
    done = turns[::-1]
    back = [done.index(k) for k in range(len(axes))]
    blocks = blocks.transpose(*back, *range(len(axes), blocks.ndim))
    return blocks.reshape(-1, *array.shape)


def whole_of(array, axes, turns, dim):
    return in_order(stacked_from(array, axes, turns), dim)


def sent_to_all(array, axis):
    length = lax.axis_size(axis)
    return lax.all_to_all(
        jnp.broadcast_to(array[None], (length, *array.shape)), axis, 0, 0, tiled=True
    )


def gathered_copies(array, axis, dim):
    blocks = sent_to_all(array, axis)
    return in_order(blocks, dim)


def norm_rows(rows, gain):
    wide = rows.astype(jnp.float32)
    scale = lax.rsqrt(jnp.mean(wide * wide, axis=-1, keepdims=True) + 1e-06)
    return (wide * scale * gain).astype(jnp.bfloat16)


def add_terms(earlier, later):
    return earlier + later


def merge_state(state, part):
    peak, total, numer = state
    new_peak, new_total, new_numer = part
    highest = jnp.maximum(peak, new_peak)
    keep = jnp.exp(peak - highest)
    fresh = jnp.exp(new_peak - highest)
    return (
        highest,
        total * keep + new_total * fresh,
        numer * keep[..., None] + new_numer * fresh[..., None],
    )


def group_partial(query, query_index, group_kv, group_bias, group, past_rows, new_rows):
    head_width = query.shape[-1]
    keys = group_kv[..., :head_width]
    values = group_kv[..., head_width:]
    score = jnp.einsum("bkgd,nkd->bkgn", query, keys, preferred_element_type=jnp.float32)
    score = score * head_width ** (-0.5) + group_bias[None]
    rank = jnp.arange(group_kv.shape[0], dtype=jnp.int32)
    new_index = group * new_rows + rank - past_rows
    visible = (rank < past_rows)[None, :] | (new_index[None, :] <= query_index[:, None])
    score = jnp.where(visible[:, None, None, :], score, -jnp.inf)
    peak = jnp.max(score, axis=-1)
    weight = jnp.exp(score - peak[..., None])
    total = jnp.sum(weight, axis=-1)
    numer = jnp.einsum(
        "bkgn,nkd->bkgd", weight.astype(jnp.bfloat16), values, preferred_element_type=jnp.float32
    )
    return (peak, total, numer)


def decode_attention(query, new_key, new_value, new_gate, cache, gate, lengths):
    seqs, pairs_here, group_size, head_width = query.shape
    span = cache.shape[1]
    keys = cache[..., :head_width]
    values = cache[..., head_width:]
    target_location = jnp.arange(span, dtype=jnp.int32)
    last_gate = jnp.sum(
        jnp.where(target_location[None, None, :] == lengths[:, None, None] - 1, gate, 0.0), axis=-1
    )
    score = jnp.einsum(
        "skgd,slkd->skgl", query, keys, preferred_element_type=jnp.float32
    ) * head_width ** (-0.5)
    score = score - gate.reshape(seqs, pairs_here, group_size, span)
    score = jnp.where(
        (target_location[None, :] < lengths[:, None])[:, None, None, :], score, -jnp.inf
    )
    own = jnp.einsum(
        "skgd,skd->skg", query, new_key, preferred_element_type=jnp.float32
    ) * head_width ** (-0.5)
    own = own - (last_gate + new_gate).reshape(seqs, pairs_here, group_size)
    peak = jnp.maximum(jnp.max(score, axis=-1), own)
    weight = jnp.exp(score - peak[..., None])
    own_weight = jnp.exp(own - peak)
    total = jnp.sum(weight, axis=-1) + own_weight
    numer = jnp.einsum(
        "skgl,slkd->skgd", weight.astype(jnp.bfloat16), values, preferred_element_type=jnp.float32
    )
    numer = numer + own_weight.astype(jnp.bfloat16).astype(jnp.float32)[..., None] * new_value[
        :, :, None, :
    ].astype(jnp.float32)
    return numer / total[..., None]


def local(
    piece_rows,
    dec_rows,
    norm_gain,
    w_query,
    w_key,
    w_value,
    w_forget,
    forget_bias,
    piece_decay,
    cache_kv,
    cache_gate,
    dec_cache,
    dec_gate,
    dec_lengths,
    w_out,
):
    piece_count = piece_rows.shape[0]
    dec_count = dec_rows.shape[0]
    past_rows = cache_kv.shape[0]
    pairs_here = cache_kv.shape[1]
    head_width = cache_kv.shape[2] // 2
    heads_here = w_forget.shape[1]
    group_size = heads_here // pairs_here
    group_rows = past_rows + piece_count
    normed = norm_rows(jnp.concatenate([piece_rows, dec_rows], axis=0), norm_gain)
    query = jnp.dot(normed, w_query, preferred_element_type=jnp.float32).astype(jnp.bfloat16)
    new_key = jnp.dot(normed, w_key, preferred_element_type=jnp.float32).astype(jnp.bfloat16)
    new_value = jnp.dot(normed, w_value, preferred_element_type=jnp.float32).astype(jnp.bfloat16)
    log_gate = jax.nn.log_sigmoid(
        jnp.dot(normed, w_forget, preferred_element_type=jnp.float32) + forget_bias
    )
    piece_gate = log_gate[:piece_count] + piece_decay.T
    running = jnp.cumsum(piece_gate, axis=0)
    before = carried_in(running[-1], KV, add_terms, jnp.zeros((heads_here,), jnp.float32))
    new_bias = -(running + before[None, :]).T
    piece_kv = jnp.concatenate(
        [
            new_key[:piece_count].reshape(piece_count, pairs_here, head_width),
            new_value[:piece_count].reshape(piece_count, pairs_here, head_width),
        ],
        axis=-1,
    )
    group_kv = jnp.concatenate([cache_kv, piece_kv], axis=0)
    group_bias = jnp.concatenate([cache_gate, new_bias], axis=1)
    my_group = lax.axis_index(KV)
    every_bias = whole_of(group_bias, KV, (0, 1), 1)
    own_query = query[:piece_count].reshape(piece_count, pairs_here, group_size, head_width)
    own_index = my_group * piece_count + jnp.arange(piece_count, dtype=jnp.int32)
    start_state = (
        jnp.full((piece_count, pairs_here, group_size), -jnp.inf, jnp.float32),
        jnp.zeros((piece_count, pairs_here, group_size), jnp.float32),
        jnp.zeros((piece_count, pairs_here, group_size, head_width), jnp.float32),
    )
    state = start_state
    piece = lax.all_gather(group_kv, KV, axis=0, tiled=True)
    count = piece.shape[0] // group_rows
    blocks = piece.reshape(count, group_rows, pairs_here, 2 * head_width)

    def visit(carry, item):
        block, offset = item
        bias = lax.dynamic_slice_in_dim(every_bias, offset * group_rows, group_rows, 1)
        part = group_partial(
            own_query,
            own_index,
            block,
            bias.reshape(pairs_here, group_size, group_rows),
            offset,
            past_rows,
            piece_count,
        )
        return (merge_state(carry, part), None)

    state, _ = lax.scan(visit, state, (blocks, jnp.arange(count, dtype=jnp.int32)))
    peak, total, numer = state
    piece_attn = numer / total[..., None]
    dec_attn = decode_attention(
        query[piece_count:].reshape(dec_count, pairs_here, group_size, head_width),
        new_key[piece_count:].reshape(dec_count, pairs_here, head_width),
        new_value[piece_count:].reshape(dec_count, pairs_here, head_width),
        log_gate[piece_count:],
        dec_cache,
        dec_gate,
        dec_lengths,
    )
    attn_rows = jnp.concatenate(
        [
            piece_attn.reshape(piece_count, heads_here * head_width),
            dec_attn.reshape(dec_count, heads_here * head_width),
        ],
        axis=0,
    ).astype(jnp.bfloat16)
    every_head = gathered_copies(attn_rows, "tp", 1)
    mixed = jnp.dot(every_head, w_out, preferred_element_type=jnp.float32).astype(jnp.bfloat16)
    return (mixed[:piece_count], mixed[piece_count:])


def solution(mesh):
    finer = Mesh(
        mesh.devices.reshape(mesh.shape["grp"], 32, 2, mesh.shape["tp"]),
        ("grp", "kv_0", "kv_1", "tp"),
    )
    return jax.shard_map(
        local,
        mesh=finer,
        in_specs=(
            P(GRP_KV, None),
            P(GRP_KV, None),
            P(),
            P(None, "tp"),
            P(None, "tp"),
            P(None, "tp"),
            P(None, "tp"),
            P("tp"),
            P("tp", GRP_KV),
            P(GRP_KV, "tp", None),
            P("tp", GRP_KV),
            P(GRP_KV, None, "tp", None),
            P(GRP_KV, "tp", None),
            P(GRP_KV),
            P(None, "tp"),
        ),
        out_specs=(P(GRP_KV, "tp"), P(GRP_KV, "tp")),
        check_vma=False,
    )
```

profile of v0, /device:TPU:33, one launch (start us, length us, event | category | flops | bytes accessed | tf_op | source)
XLA Modules:
  0.0 496.2 jit_solution(10533658309555598775)
XLA Ops:
  7.3 1.2 fusion.35
  8.6 1.4 convolution_convert_fusion.2
  10.0 1.4 convolution_convert_fusion.3
  12.3 1.7 convolution_convert_fusion.1
  14.9 96.8 %all-gather.2 = f32[64,1,4]{2,1,0:T(1,128)S(1)} all-gather(f32[1,1,4]{2,1,0:T(1,128)S(1)} %slice_bitcast_fusion.7), channel_id=1, replica_groups=mesh['grp'=2,'kv_0'=32,'kv_1'=2,'tp'=4] {'kv_0','kv_1'}, dimensions={0}, use_global_device_ids=true | all-gather | bytes 1040 | tf_op jit(solution)/shard_map/all_gather | solution.py:13
  111.8 2.6 while.31
  117.1 46.0 %all-gather.3 = f32[32,4,832]{2,1,0:T(4,128)S(1)} all-gather(f32[1,4,832]{2,1,0:T(4,128)S(1)} %maximum_bitcast_fusion), channel_id=2, replica_groups=mesh['grp'=2,'kv_0'=32,'kv_1'=2,'tp'=4] {'kv_0'}, dimensions={0}, use_global_device_ids=true | all-gather | bytes 439296 | tf_op jit(solution)/shard_map/all_gather | solution.py:33
  163.1 11.7 %all-gather.1 = f32[64,4,832]{2,1,0:T(4,128)S(1)} all-gather(f32[32,4,832]{2,1,0:T(4,128)S(1)} %all-gather.3), channel_id=3, replica_groups=mesh['grp'=2,'kv_0'=32,'kv_1'=2,'tp'=4] {'kv_1'}, dimensions={0}, use_global_device_ids=true | all-gather | bytes 1277952 | tf_op jit(solution)/shard_map/all_gather | solution.py:33
  175.6 12.4 %all-gather.6.cloned.1.call-done = bf16[53248,1,128]{2,0,1:T(8,128)(2,1)} async-done(((bf16[832,1,128]{2,0,1:T(8,128)(2,1)}), bf16[53248,1,128]{2,0,1:T(8,128)(2,1)}) %all-gather.6.cloned.1.call-update) | async-done | bytes 13631504 | tf_op jit(solution)/shard_map/all_gather | solution.py:186
  188.0 290.5 %while.32 = (s32[]{:T(128)}, f32[64,1,4]{0,2,1:T(4,128)S(1)}, f32[64,1,4]{0,2,1:T(4,128)S(1)}, f32[64,1,4,64]{0,3,2,1:T(8,128)S(1)}, s32[64]{0:T(128)S(1)}, /*in...) while((s32[]{:T(128)}, f32[64,1,4]{0,2,1:T(4,128)S(1)}, ...), condition=%wide.region_7.8_spmd.clone, body=%wide.region_4.7_spmd.clone.sunk | while | flops 56406536 | bytes 4148079 | solution.py:204
  199.2 1.0 constant_dynamic-slice_fusion.5
  221.9 1.0 constant_dynamic-slice_fusion.5
  235.5 1.0 constant_dynamic-slice_fusion.5
  271.8 1.0 constant_dynamic-slice_fusion.5
  285.4 1.0 constant_dynamic-slice_fusion.5
  308.1 1.0 constant_dynamic-slice_fusion.5
  321.8 1.0 constant_dynamic-slice_fusion.5
  358.1 1.0 constant_dynamic-slice_fusion.5
  371.7 1.0 constant_dynamic-slice_fusion.5
  394.4 1.0 constant_dynamic-slice_fusion.5
  408.0 1.0 constant_dynamic-slice_fusion.5
  444.3 1.0 constant_dynamic-slice_fusion.5
  457.9 1.0 constant_dynamic-slice_fusion.5
  478.6 9.1 %all_to_all.5 = bf16[4,66,256]{2,1,0:T(8,128)(2,1)S(1)} all-to-all(bf16[4,66,256]{2,1,0:T(8,128)(2,1)S(1)} %broadcast_in_dim.84), channel_id=1, replica_groups=mesh['grp'=2,'kv_0'=32,'kv_1'=2,'tp'=4] {'tp'}, dimensions={0} | all-to-all | bytes 270336 | tf_op jit(solution)/shard_map/all_to_all | solution.py:46
  (1027 shorter events, 197.6 us)
Async XLA Ops:
  7.2 480.7 %copy-start = (bf16[1024,512]{1,0:T(8,128)(2,1)S(1)}, bf16[1024,512]{1,0:T(8,128)(2,1)}, u32[]{:S(2)}) copy-start(bf16[1024,512]{1,0:T(8,128)(2,1)} %param.33) | copy-start | bytes 3145732
  7.2 5.1 %copy-start.6 = (bf16[2,2048]{1,0:T(2,128)(2,1)S(1)}, bf16[2,2048]{1,0:T(2,128)(2,1)}, u32[]{:S(2)}) copy-start(bf16[2,2048]{1,0:T(2,128)(2,1)} %param.20) | copy-start | bytes 24580
  7.2 5.1 %copy-start.3 = (bf16[64,2048]{1,0:T(8,128)(2,1)S(1)}, bf16[64,2048]{1,0:T(8,128)(2,1)}, u32[]{:S(2)}) copy-start(bf16[64,2048]{1,0:T(8,128)(2,1)} %param.19) | copy-start | bytes 786436
  7.2 5.1 %copy-start.10 = (f32[2048]{0:T(1024)S(1)}, f32[2048]{0:T(1024)}, u32[]{:S(2)}) copy-start(f32[2048]{0:T(1024)} %param.21) | copy-start | bytes 24580
  7.2 4.2 copy-start.4
  7.2 180.8 %all-gather.6.cloned.1.call-start = ((), (), s32[]{:S(2)}) async-start(), calls=%async_computation.1 | async-start | bytes 13844480 | tf_op jit(solution)/shard_map/all_gather | solution.py:186
  9.9 4.1 copy-start.8
  9.9 4.2 copy-start.2
  10.0 4.4 copy-start.9
  10.0 4.4 copy-start.11
  11.4 3.3 copy-start.7
  12.3 102.6 %copy-start.1 = (bf16[2,3072,1,128]{3,1,2,0:T(8,128)(2,1)S(1)}, bf16[2,3072,1,128]{3,1,2,0:T(8,128)(2,1)}, u32[]{:S(2)}) copy-start(bf16[2,3072,1,128]{3,1,2,0:T(8,128)(2,1)} %param.30) | copy-start | bytes 4718596
  115.0 2.1 copy-start.5
Sparse Core Ops, SparseCore 0:
  12.4 175.5 all-gather.5
where the time goes:
time: 499 us; the launch traced here: 496 us
  blocking collectives  164 us (33%)
  local copies, waits for them, and re-layouts  118 us (24%)
  loops' own time  90.1 us (18%)
  matrix products  64.2 us (13%)
  other arithmetic  33.3 us (7%)
  between operations  14.5 us (3%)
  waiting for transfers between devices  12.5 us (3%)
    dynamic_slice x192, local copies, waits for them, and re-layouts, local(): lax.scan(visit, state, (blocks, jnp.arange(count, dtype=jnp.int32)))  109 us
    all_gather x1, blocking collectives, carried_in(): everything = lax.all_gather(array, axis)  96.8 us
    another operation x1, loops' own time, local(): lax.scan(visit, state, (blocks, jnp.arange(count, dtype=jnp.int32)))  88.6 us
    all_gather x2, blocking collectives, stacked_from(): blocks = lax.all_gather(blocks, axes[k])  57.7 us
    dot_general x64, matrix products, group_partial(): jnp.einsum('bkgn,nkd->bkgd', weight.astype(jnp.bfloat16), values, preferr...  33.8 us
    dot_general x64, matrix products, group_partial(): jnp.einsum('bkgd,nkd->bkgn', query, keys, preferred_element_type=jnp.floa...  24 us
    reduce_sum x64, other arithmetic, group_partial(): total = jnp.sum(weight, axis=-1)  19.4 us
    all_gather x1, waiting for transfers between devices, local(): piece = lax.all_gather(group_kv, KV, axis=0, tiled=True)  12.4 us
  transfers between devices with their start and end apart: 1, of which 1 were waited for; matrix products, arithmetic and copies ran while one was open for 1% of the time, Pallas kernels for 0%

commit v1 on v0

--- a/solution.py
+++ b/solution.py
@@ -1,6 +1,8 @@
 import jax
 import jax.numpy as jnp
 from jax import lax
+from jax.experimental import pallas as pl
+from jax.experimental.pallas import tpu as pltpu
 from jax.sharding import Mesh
 from jax.sharding import PartitionSpec as P
 
@@ -63,36 +65,111 @@
     return earlier + later
 
 
-def merge_state(state, part):
-    peak, total, numer = state
-    new_peak, new_total, new_numer = part
-    highest = jnp.maximum(peak, new_peak)
-    keep = jnp.exp(peak - highest)
-    fresh = jnp.exp(new_peak - highest)
-    return (
-        highest,
-        total * keep + new_total * fresh,
-        numer * keep[..., None] + new_numer * fresh[..., None],
-    )
-
-
-def group_partial(query, query_index, group_kv, group_bias, group, past_rows, new_rows):
-    head_width = query.shape[-1]
-    keys = group_kv[..., :head_width]
-    values = group_kv[..., head_width:]
-    score = jnp.einsum("bkgd,nkd->bkgn", query, keys, preferred_element_type=jnp.float32)
-    score = score * head_width ** (-0.5) + group_bias[None]
-    rank = jnp.arange(group_kv.shape[0], dtype=jnp.int32)
-    new_index = group * new_rows + rank - past_rows
-    visible = (rank < past_rows)[None, :] | (new_index[None, :] <= query_index[:, None])
-    score = jnp.where(visible[:, None, None, :], score, -jnp.inf)
-    peak = jnp.max(score, axis=-1)
-    weight = jnp.exp(score - peak[..., None])
-    total = jnp.sum(weight, axis=-1)
-    numer = jnp.einsum(
-        "bkgn,nkd->bkgd", weight.astype(jnp.bfloat16), values, preferred_element_type=jnp.float32
-    )
-    return (peak, total, numer)
+def absorb(state, score, values):
+    peak, acc = state
+    highest = jnp.maximum(peak, jnp.max(score, axis=0, keepdims=True))
+    weight = jnp.exp(score - highest).astype(jnp.bfloat16)
+    fresh = jnp.dot(values, weight, preferred_element_type=jnp.float32)
+    return highest, acc * jnp.exp(peak - highest) + fresh
+
+
+def operands(rows, bias):
+    count, width = rows.shape
+    half = width // 2
+    pieces = bias.shape[0]
+    wide = jnp.concatenate(
+        [
+            jnp.zeros((half, count), jnp.bfloat16),
+            bias,
+            jnp.zeros((half - pieces, count), jnp.bfloat16),
+        ],
+        axis=0,
+    )
+    lane = lax.broadcasted_iota(jnp.int32, (count, width), 1)
+    keys = jnp.where(lane < half, rows, wide.T)
+    values = jnp.concatenate([rows.T[half:], jnp.ones((16, count), jnp.bfloat16)], axis=0)
+    return keys, values
+
+
+def flash_kernel(base_ref, q_ref, index_ref, kv_ref, bias_ref, fresh_ref, fresh_bias_ref, peak_ref, acc_ref):
+    step = pl.program_id(1)
+    query = q_ref[...]
+
+    @pl.when(step == 0)
+    def _():
+        peak_ref[...] = jnp.full_like(peak_ref, -jnp.inf)
+        acc_ref[...] = jnp.zeros_like(acc_ref)
+
+    state = peak_ref[...], acc_ref[...]
+    for k in range(kv_ref.shape[0]):
+        keys, values = operands(kv_ref[k], bias_ref[k])
+        score = jnp.dot(keys, query, preferred_element_type=jnp.float32)
+        state = absorb(state, score, values)
+    peak_ref[...], acc_ref[...] = state
+
+    @pl.when(step == pl.num_programs(1) - 1)
+    def _():
+        chunks, count, _ = fresh_ref.shape
+
+        def visit(k, state):
+            keys, values = operands(fresh_ref[k], fresh_bias_ref[k])
+            score = jnp.dot(keys, query, preferred_element_type=jnp.float32)
+            place = base_ref[0] + k * count + lax.broadcasted_iota(jnp.int32, score.shape, 0)
+            score = jnp.where(place <= index_ref[...], score, -jnp.inf)
+            return absorb(state, score, values)
+
+        peak_ref[...], acc_ref[...] = lax.fori_loop(0, chunks, visit, (peak_ref[...], acc_ref[...]))
+
+
+def flash(base, query, index, kv, bias, fresh, fresh_bias, past_rows, at_once, tile):
+    width, rows = query.shape
+    shards = kv.shape[0]
+    half = width // 2
+    whole = lambda array: pl.BlockSpec(array.shape, lambda r, s: (0,) * array.ndim)
+    return pl.pallas_call(
+        flash_kernel,
+        grid=(rows // tile, shards // at_once),
+        in_specs=[
+            pl.BlockSpec(memory_space=pltpu.SMEM),
+            pl.BlockSpec((width, tile), lambda r, s: (0, r)),
+            pl.BlockSpec((1, tile), lambda r, s: (0, r)),
+            pl.BlockSpec((at_once, past_rows, width), lambda r, s: (s, 0, 0)),
+            pl.BlockSpec((at_once, *bias.shape[1:]), lambda r, s: (s, 0, 0)),
+            whole(fresh),
+            whole(fresh_bias),
+        ],
+        out_specs=[
+            pl.BlockSpec((1, tile), lambda r, s: (0, r)),
+            pl.BlockSpec((half + 16, tile), lambda r, s: (0, r)),
+        ],
+        out_shape=[
+            jax.ShapeDtypeStruct((1, rows), jnp.float32),
+            jax.ShapeDtypeStruct((half + 16, rows), jnp.float32),
+        ],
+        compiler_params=pltpu.CompilerParams(
+            dimension_semantics=("arbitrary", "arbitrary"), vmem_limit_bytes=48 * 2**20
+        ),
+        name="flash",
+    )(base, query, index, kv, bias, fresh, fresh_bias)
+
+
+def bf16_pieces(array, dim):
+    first = lax.reduce_precision(array, 8, 7)
+    left = array - first
+    second = lax.reduce_precision(left, 8, 7)
+    pieces = [first, second, left - second, jnp.zeros_like(first)]
+    return jnp.concatenate(pieces, axis=dim).astype(jnp.bfloat16)
+
+
+def head_rows(query, tile_heads):
+    positions = query.shape[0]
+    width = query.shape[1] // tile_heads
+    turned = query.reshape(positions, tile_heads, width).transpose(2, 1, 0).reshape(width, -1)
+    turned = turned * jnp.asarray(width ** (-0.5), query.dtype)
+    head = jnp.arange(tile_heads * positions, dtype=jnp.int32) // positions
+    row = jnp.arange(width, dtype=jnp.int32)
+    pick = (row[:, None] % tile_heads == head[None, :]) & (row[:, None] < 3 * tile_heads)
+    return jnp.concatenate([turned, pick.astype(query.dtype)], axis=0)
 
 
 def decode_attention(query, new_key, new_value, new_gate, cache, gate, lengths):
@@ -174,36 +251,29 @@
     group_kv = jnp.concatenate([cache_kv, piece_kv], axis=0)
     group_bias = jnp.concatenate([cache_gate, new_bias], axis=1)
     my_group = lax.axis_index(KV)
-    every_bias = whole_of(group_bias, KV, (0, 1), 1)
-    own_query = query[:piece_count].reshape(piece_count, pairs_here, group_size, head_width)
-    own_index = my_group * piece_count + jnp.arange(piece_count, dtype=jnp.int32)
-    start_state = (
-        jnp.full((piece_count, pairs_here, group_size), -jnp.inf, jnp.float32),
-        jnp.zeros((piece_count, pairs_here, group_size), jnp.float32),
-        jnp.zeros((piece_count, pairs_here, group_size, head_width), jnp.float32),
-    )
-    state = start_state
-    piece = lax.all_gather(group_kv, KV, axis=0, tiled=True)
-    count = piece.shape[0] // group_rows
-    blocks = piece.reshape(count, group_rows, pairs_here, 2 * head_width)
-
-    def visit(carry, item):
-        block, offset = item
-        bias = lax.dynamic_slice_in_dim(every_bias, offset * group_rows, group_rows, 1)
-        part = group_partial(
-            own_query,
-            own_index,
-            block,
-            bias.reshape(pairs_here, group_size, group_rows),
-            offset,
-            past_rows,
-            piece_count,
-        )
-        return (merge_state(carry, part), None)
-
-    state, _ = lax.scan(visit, state, (blocks, jnp.arange(count, dtype=jnp.int32)))
-    peak, total, numer = state
-    piece_attn = numer / total[..., None]
+    every_bias = stacked_from(group_bias, KV, (0, 1))
+    gathered = lax.all_gather(group_kv, KV, axis=0, tiled=True)
+    shards = gathered.shape[0] // group_rows
+    gathered = gathered.reshape(shards, group_rows, 2 * head_width)
+    joined = 4
+    chunk = joined * piece_count
+    fresh_bias = every_bias[:, :, past_rows:].reshape(shards // joined, joined, heads_here, piece_count)
+    fresh_bias = fresh_bias.transpose(0, 2, 1, 3).reshape(shards // joined, heads_here, chunk)
+    place = my_group * piece_count + jnp.arange(piece_count, dtype=jnp.int32)
+    peak, acc = flash(
+        jnp.zeros((1,), jnp.int32),
+        head_rows(query[:piece_count], heads_here),
+        jnp.tile(place, heads_here)[None],
+        gathered,
+        bf16_pieces(every_bias[:, :, :past_rows], 1),
+        gathered[:, past_rows:].reshape(shards // joined, chunk, 2 * head_width),
+        bf16_pieces(fresh_bias, 1),
+        past_rows,
+        joined,
+        heads_here * piece_count,
+    )
+    piece_attn = acc[:head_width] / acc[head_width : head_width + 1]
+    piece_attn = piece_attn.reshape(head_width, heads_here, piece_count).transpose(2, 1, 0)
     dec_attn = decode_attention(
         query[piece_count:].reshape(dec_count, pairs_here, group_size, head_width),
         new_key[piece_count:].reshape(dec_count, pairs_here, head_width),

time: 499 us -> 252 us (0.51)
  local copies, waits for them, and re-layouts: 118 us -> 4.84 us
  loops' own time: 90.1 us -> 1.46 us
  matrix products: 64.2 us -> 6.25 us
  Pallas kernels: 0 us -> 45.3 us
  other arithmetic: 33.3 us -> 5.49 us
    dynamic_slice x256 -> x0, local copies, waits for them, and re-layouts: 114 us -> none  [the longest x192 109 us: local(): lax.scan(visit, state, (blocks, jnp.arange(count, dtype=jnp.int32)))]
    another operation x1 -> x0, loops' own time: 88.6 us -> none  [local(): lax.scan(visit, state, (blocks, jnp.arange(count, dtype=jnp.int32)))]
    dot_general x128 -> x0, matrix products: 57.8 us -> none  [the longest x64 33.8 us: group_partial(): jnp.einsum('bkgn,nkd->bkgd', weight.astype(jnp.bfloat16), values, preferr...]
    pallas_call x0 -> x1, Pallas kernels: none -> 45.3 us  [flash(): pl.pallas_call(flash_kernel, grid=(rows // tile, shards // at_once), in_s...]
    reduce_sum x64 -> x0, other arithmetic: 19.4 us -> none  [group_partial(): total = jnp.sum(weight, axis=-1)]
    or x64 -> x0, other arithmetic: 6.8 us -> none  [group_partial(): (rank < past_rows)[None, :] | (new_index[None, :] <= query_index[:, None])]
  transfers between devices with their start and end apart: 1 -> 1, of which waited for: 1 -> 1; matrix products, arithmetic and copies ran while one was open for 1% -> 3% of each run, Pallas kernels for 0% -> 0%
where the time goes in v1:
time: 252 us
  blocking collectives  163 us (65%)
  Pallas kernels  45.3 us (18%)
  between operations  14.5 us (6%)
  waiting for transfers between devices  11 us (4%)
  matrix products  6.25 us (2%)
  other arithmetic  5.49 us (2%)
  local copies, waits for them, and re-layouts  4.84 us (2%)
    all_gather x1, blocking collectives, carried_in(): everything = lax.all_gather(array, axis)  96.9 us
    all_gather x2, blocking collectives, stacked_from(): blocks = lax.all_gather(blocks, axes[k])  57.7 us
    pallas_call x1, Pallas kernels, flash(): pl.pallas_call(flash_kernel, grid=(rows // tile, shards // at_once), in_s...  45.3 us
    all_gather x1, waiting for transfers between devices, local(): gathered = lax.all_gather(group_kv, KV, axis=0, tiled=True)  10.9 us
    all_to_all x1, blocking collectives, sent_to_all(): lax.all_to_all(jnp.broadcast_to(array[None], (length, *array.shape)), axi...  8.33 us
  transfers between devices with their start and end apart: 1, of which 1 were waited for; matrix products, arithmetic and copies ran while one was open for 3% of the time, Pallas kernels for 0%

profile of v1, /device:TPU:33, one launch (start us, length us, event | category | flops | bytes accessed | tf_op | source)
XLA Modules:
  0.0 251.7 jit_solution(1534474687325132894)
XLA Ops:
  7.3 1.3 fusion.18
  8.6 1.4 convolution_convert_fusion.3
  10.0 1.4 convolution_convert_fusion.2
  11.4 0.8 maximum_maximum_fusion.1
  12.5 0.1 select_reduce_fusion
  12.7 0.3 fusion.26
  13.3 96.9 %all-gather.2 = f32[64,1,4]{2,1,0:T(1,128)S(1)} all-gather(f32[1,1,4]{2,1,0:T(1,128)S(1)} %slice_bitcast_fusion.3), channel_id=1, replica_groups=mesh['grp'=2,'kv_0'=32,'kv_1'=2,'tp'=4] {'kv_0','kv_1'}, dimensions={0}, use_global_device_ids=true | all-gather | bytes 1040 | tf_op jit(solution)/shard_map/all_gather | solution.py:15
  110.1 2.6 %while.14 = (s32[]{:T(128)}, f32[4]{0:T(128)S(1)}, s32[]{:T(128)}, f32[64,4]{1,0:T(8,128)S(1)}, s32[]{:T(128)}, /*index=5*/s32[]{:T(128)}) while((s32[]{:T(128)}, f32[4]{0:T(128)S(1)}, s32[]{:T(128)}, f32[64,4]{1,0:T(8,128)S(1)}, s32[]{:T(128)}, /*index=5*/s32[]{:T(128)}) %tuple.49), condition=%wide.region_3.4_spmd.clone, body=%wide.region_2.3_spmd.clone.sunk | while | flops 16 | bytes 149 | solution.py:23
  112.8 1.6 convolution_convert_fusion.1
  115.2 0.6 fusion.36
  116.1 0.2 fusion.21
  116.5 0.6 fusion.13
  117.3 46.7 %all-gather.3 = f32[32,4,832]{2,1,0:T(4,128)S(1)} all-gather(f32[1,4,832]{2,1,0:T(4,128)S(1)} %maximum_bitcast_fusion), channel_id=2, replica_groups=mesh['grp'=2,'kv_0'=32,'kv_1'=2,'tp'=4] {'kv_0'}, dimensions={0}, use_global_device_ids=true | all-gather | bytes 439296 | tf_op jit(solution)/shard_map/all_gather | solution.py:35
  164.0 10.9 %all-gather.1 = f32[64,4,832]{2,1,0:T(4,128)S(1)} all-gather(f32[32,4,832]{2,1,0:T(4,128)S(1)} %all-gather.3), channel_id=3, replica_groups=mesh['grp'=2,'kv_0'=32,'kv_1'=2,'tp'=4] {'kv_1'}, dimensions={0}, use_global_device_ids=true | all-gather | bytes 1277952 | tf_op jit(solution)/shard_map/all_gather | solution.py:35
  175.1 0.1 reshape.217
  175.6 0.4 reduce-precision_convert_fusion.1
  176.0 0.9 maximum_maximum_fusion.bias_ref
  176.9 10.9 %all-gather.6.cloned.1.call-done = bf16[53248,1,128]{2,0,1:T(8,128)(2,1)} async-done(((bf16[832,1,128]{2,0,1:T(8,128)(2,1)}), bf16[53248,1,128]{2,0,1:T(8,128)(2,1)}) %all-gather.6.cloned.1.call-update) | async-done | bytes 13631504 | tf_op jit(solution)/shard_map/all_gather | solution.py:255
  187.9 1.3 slice.77
  189.2 45.3 %flash.1 = (f32[1,256]{1,0:T(1,128)}, f32[80,256]{1,0:T(8,128)S(1)}) custom-call(s32[1]{0:T(128)} %constant.80.clone.1.base_ref, bf16[128,256]{1,0:T(8,128)(2,1)S(1)} %pad_maximum_fusion.1.q_ref, s32[1,256]{1,0:T(1,128)S(1)} %broadcast_in_dim_tile.3.index_ref, bf16[64,832,128]{2,1,0:T(8,128)(2,1)} %bitcast.67, ...), custom_call_target="tpu_custom_call" | custom-call | tf_op jit(solution)/shard_map/flash/pallas_call | solution.py:129
  234.8 8.3 %all_to_all.5 = bf16[4,66,256]{2,1,0:T(8,128)(2,1)S(1)} all-to-all(bf16[4,66,256]{2,1,0:T(8,128)(2,1)S(1)} %broadcast_in_dim.36), channel_id=1, replica_groups=mesh['grp'=2,'kv_0'=32,'kv_1'=2,'tp'=4] {'tp'}, dimensions={0} | all-to-all | bytes 270336 | tf_op jit(solution)/shard_map/all_to_all | solution.py:48
  243.3 0.3 convolution_convert_fusion
  243.6 0.6 slice.83
  244.2 0.6 slice.82
  (147 shorter events, 4.2 us)
Async XLA Ops:
  7.2 236.2 %copy-start = (bf16[1024,512]{1,0:T(8,128)(2,1)S(1)}, bf16[1024,512]{1,0:T(8,128)(2,1)}, u32[]{:S(2)}) copy-start(bf16[1024,512]{1,0:T(8,128)(2,1)} %param.31) | copy-start | bytes 3145732
  7.2 5.5 %copy-start.6 = (bf16[2,2048]{1,0:T(2,128)(2,1)S(1)}, bf16[2,2048]{1,0:T(2,128)(2,1)}, u32[]{:S(2)}) copy-start(bf16[2,2048]{1,0:T(2,128)(2,1)} %param.18) | copy-start | bytes 24580
  7.2 5.5 %copy-start.3 = (bf16[64,2048]{1,0:T(8,128)(2,1)S(1)}, bf16[64,2048]{1,0:T(8,128)(2,1)}, u32[]{:S(2)}) copy-start(bf16[64,2048]{1,0:T(8,128)(2,1)} %param.17) | copy-start | bytes 786436
  7.2 5.5 %copy-start.10 = (f32[2048]{0:T(1024)S(1)}, f32[2048]{0:T(1024)}, u32[]{:S(2)}) copy-start(f32[2048]{0:T(1024)} %param.19) | copy-start | bytes 24580
  7.2 4.2 %copy-start.4 = (bf16[768,1,128]{2,0,1:T(8,128)(2,1)S(1)}, bf16[768,1,128]{2,0,1:T(8,128)(2,1)}, u32[]{:S(2)}) copy-start(bf16[768,1,128]{2,0,1:T(8,128)(2,1)} %param.26) | copy-start | bytes 589828
  7.2 5.1 %copy-start.8 = (s32[2]{0:T(128)S(1)}, s32[2]{0:T(128)}, u32[]{:S(2)}) copy-start(s32[2]{0:T(128)} %param.30) | copy-start | bytes 28
  7.3 5.2 %copy-start.2 = (f32[2,4,3072]{2,1,0:T(4,128)S(1)}, f32[2,4,3072]{2,1,0:T(4,128)}, u32[]{:S(2)}) copy-start(f32[2,4,3072]{2,1,0:T(4,128)} %param.29) | copy-start | bytes 294916
  7.3 5.5 %copy-start.11 = (f32[4]{0:T(128)S(1)}, f32[4]{0:T(128)}, u32[]{:S(2)}) copy-start(f32[4]{0:T(128)} %param.24) | copy-start | bytes 52
  7.3 5.5 %copy-start.9 = (bf16[2048,4]{0,1:T(4,128)(2,1)S(1)}, bf16[2048,4]{0,1:T(4,128)(2,1)}, u32[]{:S(2)}) copy-start(bf16[2048,4]{0,1:T(4,128)(2,1)} %param.23) | copy-start | bytes 49156
  7.3 180.6 %all-gather.6.cloned.1.call-start = ((), (), s32[]{:S(2)}) async-start(), calls=%async_computation.1 | async-start | bytes 13844480 | tf_op jit(solution)/shard_map/all_gather | solution.py:255
  10.0 3.0 %copy-start.7 = (f32[4,64]{1,0:T(4,128)S(1)}, f32[4,64]{1,0:T(4,128)}, u32[]{:S(2)}) copy-start(f32[4,64]{1,0:T(4,128)} %param.25) | copy-start | bytes 3076
  12.7 102.4 %copy-start.1 = (bf16[2,3072,1,128]{3,1,2,0:T(8,128)(2,1)S(1)}, bf16[2,3072,1,128]{3,1,2,0:T(8,128)(2,1)}, u32[]{:S(2)}) copy-start(bf16[2,3072,1,128]{3,1,2,0:T(8,128)(2,1)} %param.28) | copy-start | bytes 4718596
  115.1 2.1 copy-start.5
Sparse Core Ops, SparseCore 0:
  12.4 175.4 all-gather.5

commit v2 on v1

v2 whole, which is shorter than its diff:
```python
import functools

import jax
import jax.numpy as jnp
from jax import lax
from jax.experimental import pallas as pl
from jax.experimental.pallas import tpu as pltpu
from jax.sharding import Mesh
from jax.sharding import PartitionSpec as P

GRP_KV = ("grp", "run", "near", "core")
PIECES = 3
SPARE = 8


def to_each(array, axis):
    members = lax.axis_size(axis)
    return lax.all_to_all(
        jnp.broadcast_to(array[None], (members, *array.shape)), axis, 0, 0, tiled=True
    )


def norm_rows(rows, gain):
    wide = rows.astype(jnp.float32)
    scale = lax.rsqrt(jnp.mean(wide * wide, axis=-1, keepdims=True) + 1e-06)
    return (wide * scale * gain).astype(jnp.bfloat16)


def absorb(state, score, values):
    peak, acc = state
    highest = jnp.maximum(peak, jnp.max(score, axis=0, keepdims=True))
    weight = jnp.exp(score - highest).astype(jnp.bfloat16)
    fresh = jnp.dot(values, weight, preferred_element_type=jnp.float32)
    return highest, acc * jnp.exp(peak - highest) + fresh


def operands(rows, bias):
    count, width = rows.shape
    half = width // 2
    pieces = bias.shape[0]
    wide = jnp.concatenate(
        [
            jnp.zeros((half, count), jnp.bfloat16),
            bias,
            jnp.zeros((half - pieces, count), jnp.bfloat16),
        ],
        axis=0,
    )
    lane = lax.broadcasted_iota(jnp.int32, (count, width), 1)
    keys = jnp.where(lane < half, rows, wide.T)
    values = jnp.concatenate([rows.T[half:], jnp.ones((16, count), jnp.bfloat16)], axis=0)
    return keys, values


def cut(array):
    first = array.astype(jnp.bfloat16).astype(jnp.float32)
    left = array - first
    second = left.astype(jnp.bfloat16).astype(jnp.float32)
    return [first, second, left - second]


def query_tile(q_ref, first_head, heads):
    members, width, lanes = q_ref.shape
    turned = jnp.concatenate([q_ref[k] for k in range(members)], axis=1)
    each = lanes // (heads // 2)
    shape = (width, members * lanes)
    row = lax.broadcasted_iota(jnp.int32, shape, 0)
    head = first_head + lax.broadcasted_iota(jnp.int32, shape, 1) % lanes // each
    pick = (row % heads == head) & (row < PIECES * heads)
    return jnp.concatenate([turned, pick.astype(jnp.float32).astype(jnp.bfloat16)], axis=0)


def past_kernel(first_head, heads, q_ref, mine_ref, other_ref, mine_bias_ref, other_bias_ref, peak_ref, acc_ref):
    query = query_tile(q_ref, first_head, heads)

    @pl.when(pl.program_id(1) == 0)
    def _():
        peak_ref[...] = jnp.full_like(peak_ref, -jnp.inf)
        acc_ref[...] = jnp.zeros_like(acc_ref)

    state = peak_ref[...], acc_ref[...]
    for kv_ref, bias_ref in ((mine_ref, mine_bias_ref), (other_ref, other_bias_ref)):
        for k in range(kv_ref.shape[0]):
            keys, values = operands(kv_ref[k], bias_ref[k])
            score = jnp.dot(keys, query, preferred_element_type=jnp.float32)
            state = absorb(state, score, values)
    peak_ref[...], acc_ref[...] = state


def fresh_kernel(first_head, heads, place_ref, q_ref, kv_ref, bias_ref, peak_ref, acc_ref, out_ref):
    query = query_tile(q_ref, first_head, heads)
    width, tile = query.shape
    half = width // 2
    members, _, lanes = out_ref.shape
    each = lanes // (heads // 2)
    chunks, count, _ = kv_ref.shape
    state = peak_ref[...], acc_ref[...]
    lane = lax.broadcasted_iota(jnp.int32, (1, tile), 1)
    member = pl.program_id(0) * members + lane // lanes
    asked = member * (chunks * count) + place_ref[0] + lane % each
    for k in range(chunks):
        keys, values = operands(kv_ref[k], bias_ref[k])
        score = jnp.dot(keys, query, preferred_element_type=jnp.float32)
        place = place_ref[1] + k * count + lax.broadcasted_iota(jnp.int32, score.shape, 0)
        score = jnp.where(place <= asked, score, -jnp.inf)
        state = absorb(state, score, values)
    peak, acc = state
    rows = [acc[:half], *cut(peak), *cut(acc[half : half + 1])]
    rows.append(jnp.zeros((SPARE - 2 * PIECES, tile), jnp.float32))
    sent = jnp.concatenate(rows, axis=0).astype(jnp.bfloat16)
    for k in range(members):
        out_ref[k] = sent[:, k * lanes : (k + 1) * lanes]


def attend(side, places, queries, mine, other, mine_bias, other_bias, fresh, fresh_bias, past_rows, heads):
    members, _, lanes = queries.shape
    shards, _, width = mine.shape
    half = width // 2
    at_once, joined = 2, 2
    tile = joined * lanes
    rows = members * lanes
    whole = lambda array: pl.BlockSpec(array.shape, lambda *_: (0,) * array.ndim)
    shard = lambda count: pl.BlockSpec((at_once, count, width), lambda r, s: (s, 0, 0))
    bias_block = pl.BlockSpec((at_once, *mine_bias.shape[1:]), lambda r, s: (s, 0, 0))
    first_head = side * (heads // 2)
    work = 2 * shards * past_rows * rows
    peak, acc = pl.pallas_call(
        functools.partial(past_kernel, first_head, heads),
        grid=(members // joined, shards // at_once),
        in_specs=[
            pl.BlockSpec((joined, half, lanes), lambda r, s: (r, side, 0)),
            shard(past_rows),
            shard(past_rows),
            bias_block,
            bias_block,
        ],
        out_specs=[
            pl.BlockSpec((1, tile), lambda r, s: (0, r)),
            pl.BlockSpec((half + 16, tile), lambda r, s: (0, r)),
        ],
        out_shape=[
            jax.ShapeDtypeStruct((1, rows), jnp.float32),
            jax.ShapeDtypeStruct((half + 16, rows), jnp.float32),
        ],
        compiler_params=pltpu.CompilerParams(
            dimension_semantics=("arbitrary", "arbitrary"), vmem_limit_bytes=40 * 2**20
        ),
        cost_estimate=pl.CostEstimate(
            flops=work * width * 2, transcendentals=work, bytes_accessed=4 * mine.size
        ),
        name="past",
    )(queries, mine, other, mine_bias, other_bias)
    return pl.pallas_call(
        functools.partial(fresh_kernel, first_head, heads),
        grid=(members // joined,),
        in_specs=[
            pl.BlockSpec(memory_space=pltpu.SMEM),
            pl.BlockSpec((joined, half, lanes), lambda r: (r, side, 0)),
            whole(fresh),
            whole(fresh_bias),
            pl.BlockSpec((1, tile), lambda r: (0, r)),
            pl.BlockSpec((half + 16, tile), lambda r: (0, r)),
        ],
        out_specs=pl.BlockSpec((joined, half + SPARE, lanes), lambda r: (r, 0, 0)),
        out_shape=jax.ShapeDtypeStruct((members, half + SPARE, lanes), jnp.bfloat16),
        compiler_params=pltpu.CompilerParams(
            dimension_semantics=("arbitrary",), vmem_limit_bytes=32 * 2**20
        ),
        cost_estimate=pl.CostEstimate(
            flops=fresh.shape[0] * fresh.shape[1] * rows * width * 4,
            transcendentals=fresh.shape[0] * fresh.shape[1] * rows,
            bytes_accessed=4 * acc.size,
        ),
        name="fresh",
    )(places, queries, fresh, fresh_bias, peak, acc)


def bf16_pieces(array, dim):
    first = lax.reduce_precision(array, 8, 7)
    left = array - first
    second = lax.reduce_precision(left, 8, 7)
    return jnp.concatenate([first, second, left - second], axis=dim).astype(jnp.bfloat16)


def bias_rows(bias):
    pieces = bf16_pieces(bias, -2)
    spare = jnp.zeros((*pieces.shape[:-2], 16 - pieces.shape[-2], pieces.shape[-1]), jnp.bfloat16)
    return jnp.concatenate([pieces, spare], axis=-2)


def packed(array, lanes):
    flat = array.reshape(-1)
    rows = -(-flat.shape[0] // lanes)
    return jnp.pad(flat, (0, rows * lanes - flat.shape[0])).reshape(rows, lanes)


def merged(parts, half):
    wide = parts.astype(jnp.float32)
    peak = wide[:, half] + wide[:, half + 1] + wide[:, half + 2]
    total = wide[:, half + 3] + wide[:, half + 4] + wide[:, half + 5]
    share = jnp.exp(peak - jnp.max(peak, axis=0))
    numer = jnp.sum(wide[:, :half] * share[:, None, :], axis=0)
    return numer / jnp.sum(total * share, axis=0)


def decode_attention(query, new_key, new_value, new_gate, cache, gate, lengths):
    seqs, pairs_here, group_size, head_width = query.shape
    span = cache.shape[1]
    keys = cache[..., :head_width]
    values = cache[..., head_width:]
    target_location = jnp.arange(span, dtype=jnp.int32)
    last_gate = jnp.sum(
        jnp.where(target_location[None, None, :] == lengths[:, None, None] - 1, gate, 0.0), axis=-1
    )
    score = jnp.einsum(
        "skgd,slkd->skgl", query, keys, preferred_element_type=jnp.float32
    ) * head_width ** (-0.5)
    score = score - gate.reshape(seqs, pairs_here, group_size, span)
    score = jnp.where(
        (target_location[None, :] < lengths[:, None])[:, None, None, :], score, -jnp.inf
    )
    own = jnp.einsum(
        "skgd,skd->skg", query, new_key, preferred_element_type=jnp.float32
    ) * head_width ** (-0.5)
    own = own - (last_gate + new_gate).reshape(seqs, pairs_here, group_size)
    peak = jnp.maximum(jnp.max(score, axis=-1), own)
    weight = jnp.exp(score - peak[..., None])
    own_weight = jnp.exp(own - peak)
    total = jnp.sum(weight, axis=-1) + own_weight
    numer = jnp.einsum(
        "skgl,slkd->skgd", weight.astype(jnp.bfloat16), values, preferred_element_type=jnp.float32
    )
    numer = numer + own_weight.astype(jnp.bfloat16).astype(jnp.float32)[..., None] * new_value[
        :, :, None, :
    ].astype(jnp.float32)
    return numer / total[..., None]


def step(
    piece_rows,
    dec_rows,
    norm_gain,
    w_query,
    w_key,
    w_value,
    w_forget,
    forget_bias,
    piece_decay,
    cache_kv,
    cache_gate,
    dec_cache,
    dec_gate,
    dec_lengths,
    w_out,
):
    piece_count = piece_rows.shape[0]
    dec_count = dec_rows.shape[0]
    past_rows, pairs_here, width = cache_kv.shape
    head_width = width // 2
    heads_here = w_forget.shape[1]
    group_size = heads_here // pairs_here
    lanes = heads_here // 2 * piece_count
    neighbours = lax.axis_size(("near", "core"))
    me = lax.axis_index(("near", "core"))
    run = lax.axis_index("run")

    past_bias = bias_rows(cache_gate)
    past = jnp.concatenate([cache_kv[:, 0], past_bias.reshape(-1, width)], axis=0)
    mine = to_each(past, "near")

    normed = norm_rows(jnp.concatenate([piece_rows, dec_rows], axis=0), norm_gain)
    query = jnp.dot(normed, w_query, preferred_element_type=jnp.float32).astype(jnp.bfloat16)
    new_key = jnp.dot(normed, w_key, preferred_element_type=jnp.float32).astype(jnp.bfloat16)
    new_value = jnp.dot(normed, w_value, preferred_element_type=jnp.float32).astype(jnp.bfloat16)
    log_gate = jax.nn.log_sigmoid(
        jnp.dot(normed, w_forget, preferred_element_type=jnp.float32) + forget_bias
    )
    running = jnp.cumsum(log_gate[:piece_count].T + piece_decay, axis=1)

    scaled = query[:piece_count] * jnp.asarray(head_width ** (-0.5), query.dtype)
    turned = scaled.reshape(piece_count, 2, heads_here // 2, head_width).transpose(1, 3, 2, 0)
    asked = jnp.concatenate(
        [
            turned.reshape(2 * head_width, lanes),
            packed(bf16_pieces(running[None, :, -1], 0), lanes),
            jnp.zeros((SPARE - 1, lanes), jnp.bfloat16),
        ],
        axis=0,
    )
    asked, mine = lax.optimization_barrier((asked, mine))
    queries = to_each(asked, "run")
    other = lax.ppermute(mine, "core", [(0, 1), (1, 0)])
    mine_bias, other_bias = (
        block[:, past_rows:].reshape(-1, *past_bias.shape) for block in (mine, other)
    )
    totals = queries[:, 2 * head_width, : PIECES * heads_here].astype(jnp.float32)
    totals = totals.reshape(-1, PIECES, heads_here).sum(1)
    earlier = jnp.arange(totals.shape[0], dtype=jnp.int32)[:, None] < run
    earlier = jnp.sum(jnp.where(earlier, totals, 0.0), axis=0)

    own = jnp.concatenate(
        [
            jnp.concatenate([new_key[:piece_count], new_value[:piece_count]], axis=1),
            packed(bf16_pieces(running[None], 0), width),
            packed(bf16_pieces(earlier[None], 0), width),
        ],
        axis=0,
    )
    own = jnp.pad(own, ((0, -own.shape[0] % SPARE), (0, 0)))
    dec_attn = decode_attention(
        query[piece_count:].reshape(dec_count, pairs_here, group_size, head_width),
        new_key[piece_count:].reshape(dec_count, pairs_here, head_width),
        new_value[piece_count:].reshape(dec_count, pairs_here, head_width),
        log_gate[piece_count:],
        dec_cache,
        dec_gate,
        dec_lengths,
    )
    own, dec_attn = lax.optimization_barrier((own, dec_attn))
    news = to_each(own, ("near", "core"))
    run_rows = PIECES * heads_here * piece_count // width
    ran = news[:, piece_count : piece_count + run_rows].astype(jnp.float32)
    ran = ran.reshape(neighbours, PIECES, heads_here, piece_count).sum(1)
    before = news[:, piece_count + run_rows, : PIECES * heads_here].astype(jnp.float32)
    before = before.reshape(neighbours, PIECES, heads_here).sum((0, 1))
    ends = ran[:, :, -1]
    before = before + jnp.cumsum(ends, axis=0) - ends
    joined = 4
    chunks = neighbours // joined
    fresh_bias = -(ran + before[:, :, None])
    fresh_bias = fresh_bias.reshape(chunks, joined, heads_here, piece_count).transpose(0, 2, 1, 3)
    fresh_bias = bias_rows(fresh_bias.reshape(chunks, heads_here, joined * piece_count))
    fresh = news[:, :piece_count].reshape(chunks, joined * piece_count, width)
    places = jnp.stack([me, run * neighbours]).astype(jnp.int32) * piece_count

    backs = []
    asking = queries
    for side in range(2):
        sent = attend(
            side, places, asking, mine, other, mine_bias, other_bias, fresh, fresh_bias, past_rows, heads_here
        )
        asking, sent, backs = lax.optimization_barrier((asking, sent, backs))
        backs = [*backs, lax.all_to_all(sent, "run", 0, 0, tiled=True)]
    columns = []
    for back in backs:
        part = merged(back, head_width).reshape(head_width, heads_here // 2, piece_count)
        columns.append(part.transpose(2, 1, 0).reshape(piece_count, -1))
    attn_rows = jnp.concatenate(
        [jnp.concatenate(columns, axis=1), dec_attn.reshape(dec_count, heads_here * head_width)],
        axis=0,
    ).astype(jnp.bfloat16)
    every_head = jnp.moveaxis(to_each(attn_rows, "tp"), 0, 1).reshape(attn_rows.shape[0], -1)
    mixed = jnp.dot(every_head, w_out, preferred_element_type=jnp.float32).astype(jnp.bfloat16)
    return (mixed[:piece_count], mixed[piece_count:])


def solution(mesh):
    near, core = 4, 2
    grp, kv, tp = (mesh.shape[axis] for axis in ("grp", "kv", "tp"))
    finer = Mesh(
        mesh.devices.reshape(grp, kv // (near * core), near, core, tp),
        ("grp", "run", "near", "core", "tp"),
    )
    return jax.shard_map(
        step,
        mesh=finer,
        in_specs=(
            P(GRP_KV, None),
            P(GRP_KV, None),
            P(),
            P(None, "tp"),
            P(None, "tp"),
            P(None, "tp"),
            P(None, "tp"),
            P("tp"),
            P("tp", GRP_KV),
            P(GRP_KV, "tp", None),
            P("tp", GRP_KV),
            P(GRP_KV, None, "tp", None),
            P(GRP_KV, "tp", None),
            P(GRP_KV),
            P(None, "tp"),
        ),
        out_specs=(P(GRP_KV, "tp"), P(GRP_KV, "tp")),
        check_vma=False,
    )
```

time: 252 us -> 240 us (0.952); the launches traced: 252 us -> 236 us
  blocking collectives: 163 us -> 9.02 us
  starting transfers between devices: 0.06 us -> 93.7 us
  waiting for transfers between devices: 11 us -> 63.8 us
  between operations: 14.5 us -> 1.22 us
  local copies, waits for them, and re-layouts: 4.84 us -> 10.6 us
    all_gather x3 -> x0, blocking collectives: 155 us -> none  [the longest x1 96.9 us: carried_in(): everything = lax.all_gather(array, axis)]
    all_to_all x0 -> x5, starting transfers between devices: none -> 90.1 us  [the longest x3 71 us: to_each(): lax.all_to_all(jnp.broadcast_to(array[None], (members, *array.shape)), ax...]
    all_to_all x0 -> x5, waiting for transfers between devices: none -> 63.8 us  [the longest x3 32 us: to_each(): lax.all_to_all(jnp.broadcast_to(array[None], (members, *array.shape)), ax...]
    all_gather x1 -> x0, waiting for transfers between devices: 10.9 us -> none  [local(): gathered = lax.all_gather(group_kv, KV, axis=0, tiled=True)]
    ppermute x0 -> x1, starting transfers between devices: none -> 3.61 us  [step(): other = lax.ppermute(mine, 'core', [(0, 1), (1, 0)])]
    pallas_call x1 -> x4, Pallas kernels: 45.3 us -> 45.9 us  [the longest x2 37.7 us: attend(): pl.pallas_call(functools.partial(past_kernel, first_head, heads), grid=(m...]
  transfers between devices with their start and end apart: 1 -> 6, of which waited for: 1 -> 4; matrix products, arithmetic and copies ran while one was open for 3% -> 5% of each run, Pallas kernels for 0% -> 18%
where the time goes in v2:
time: 240 us; the launch traced here: 236 us
  starting transfers between devices  93.7 us (39%)
  waiting for transfers between devices  63.8 us (27%)
  Pallas kernels  45.9 us (19%)
  local copies, waits for them, and re-layouts  10.6 us (4%)
  blocking collectives  9.02 us (4%)
  matrix products  6.91 us (3%)
  other arithmetic  4.73 us (2%)
    all_to_all x3, starting transfers between devices, to_each(): lax.all_to_all(jnp.broadcast_to(array[None], (members, *array.shape)), ax...  71 us
    pallas_call x2, Pallas kernels, attend(): pl.pallas_call(functools.partial(past_kernel, first_head, heads), grid=(m...  37.7 us
    all_to_all x3, waiting for transfers between devices, to_each(): lax.all_to_all(jnp.broadcast_to(array[None], (members, *array.shape)), ax...  32 us
    all_to_all x2, waiting for transfers between devices, step(): backs = [*backs, lax.all_to_all(sent, 'run', 0, 0, tiled=True)]  31.8 us
    all_to_all x2, starting transfers between devices, step(): backs = [*backs, lax.all_to_all(sent, 'run', 0, 0, tiled=True)]  19.1 us
    all_to_all x1, blocking collectives, to_each(): lax.all_to_all(jnp.broadcast_to(array[None], (members, *array.shape)), ax...  9.02 us
    pallas_call x2, Pallas kernels, attend(): pl.pallas_call(functools.partial(fresh_kernel, first_head, heads), grid=(...  8.21 us
  transfers between devices with their start and end apart: 6, of which 4 were waited for; matrix products, arithmetic and copies ran while one was open for 5% of the time, Pallas kernels for 18%

profile of v2, /device:TPU:33, one launch (start us, length us, event | category | flops | bytes accessed | tf_op | source)
XLA Modules:
  0.0 235.9 jit_solution(13259211705760456702)
XLA Ops:
  1.6 1.0 pad_maximum_fusion.1
  2.6 1.0 broadcast_in_dim.47
  3.6 9.2 %all-to-all-start = ((bf16[4,864,128]{2,1,0:T(8,128)(2,1)}), bf16[4,864,128]{2,1,0:T(8,128)(2,1)S(1)}, u32[]{:S(2)}, u32[]{:S(2)}) async-start(bf16[4,864,128]{2,1,0:T(8,128)(2,1)} %broadcast_in_dim.47), calls=%async_computation | async-start | bytes 1769472 | tf_op jit(solution)/shard_map/all_to_all | solution.py:18
  14.9 1.6 convolution_convert_fusion.1
  17.4 8.4 %all-to-all-done.mine_ref = bf16[4,864,128]{2,1,0:T(8,128)(2,1)S(1)} async-done(((bf16[4,864,128]{2,1,0:T(8,128)(2,1)}), bf16[4,864,128]{2,1,0:T(8,128)(2,1)S(1)}, u32[]{:S(2)}, u32[]{:S(2)}) %all-to-all-start) | async-done | bytes 884768 | tf_op jit(solution)/shard_map/all_to_all | solution.py:18
  26.5 49.2 %all-to-all-start.1 = ((bf16[8,136,128]{2,1,0:T(8,128)(2,1)}), bf16[8,136,128]{2,1,0:T(8,128)(2,1)S(1)}, u32[]{:S(2)}, u32[]{:S(2)}) async-start(bf16[8,136,128]{2,1,0:T(8,128)(2,1)} %broadcast_in_dim.48), calls=%async_computation.1 | async-start | bytes 557056 | tf_op jit(solution)/shard_map/all_to_all | solution.py:18
  75.9 2.0 fusion.73
  78.7 2.0 fusion.14
  80.7 3.6 %collective-permute-start = (bf16[4,864,128]{2,1,0:T(8,128)(2,1)S(1)}, bf16[4,864,128]{2,1,0:T(8,128)(2,1)S(1)}, u32[]{:S(2)}, u32[]{:S(2)}) collective-permute-start(bf16[4,864,128]{2,1,0:T(8,128)(2,1)S(1)} %all-to-all-done.mine_ref), channel_id=1, source_target_pairs={{0,4},{4,0},{1,5},{5,1},{2,6},{6,2},{3,7},{7,3},{8,12},{12,8},{9,1... | collective-permute-start | bytes 2654216 | tf_op jit(solution)/shard_map/ppermute | solution.py:292
  84.3 23.6 %all-to-all-done.1.q_ref = bf16[8,136,128]{2,1,0:T(8,128)(2,1)S(1)} async-done(((bf16[8,136,128]{2,1,0:T(8,128)(2,1)}), bf16[8,136,128]{2,1,0:T(8,128)(2,1)S(1)}, u32[]{:S(2)}, u32[]{:S(2)}) %all-to-all-start.1) | async-done | bytes 278560 | tf_op jit(solution)/shard_map/all_to_all | solution.py:18
  109.0 12.5 %all-to-all-start.2 = ((bf16[8,72,128]{2,1,0:T(8,128)(2,1)}), bf16[8,72,128]{2,1,0:T(8,128)(2,1)S(1)}, u32[]{:S(2)}, u32[]{:S(2)}) async-start(bf16[8,72,128]{2,1,0:T(8,128)(2,1)} %broadcast_in_dim.55), calls=%async_computation.2 | async-start | bytes 294912 | tf_op jit(solution)/shard_map/all_to_all | solution.py:18
  121.9 18.8 %past.2 = (f32[1,1024]{1,0:T(1,128)S(1)}, f32[80,1024]{1,0:T(8,128)S(1)}) custom-call(bf16[8,136,128]{2,1,0:T(8,128)(2,1)S(1)} %all-to-all-done.1.q_ref, bf16[4,864,128]{2,1,0:T(8,128)(2,1)S(1)} %all-to-all-done.mine_ref, bf16[4,864,128]{2,1,0:T(8,128)(2,1)S(1)} %collective-permute-done.other_ref, bf16[4,16,768]{2,1,0:T(8,128)(2,1)S(1)} %reshape.384.mine_bias_ref, ...), custom_call_target="tpu_custom_call" | custom-call | flops 1610612736 | bytes 1769472 | tf_op jit(solution)/shard_map/past/pallas_call | solution.py:127
  142.3 0.9 slice.143
  143.2 1.0 copy-done.2
  144.2 4.1 %fresh.2 = bf16[8,72,128]{2,1,0:T(8,128)(2,1)} custom-call(s32[2]{0:T(128)S(1)} %add_multiply_fusion.place_ref, bf16[8,136,128]{2,1,0:T(8,128)(2,1)S(1)} %all-to-all-done.1.q_ref, bf16[2,256,128]{2,1,0:T(8,128)(2,1)S(1)} %bitcast.112, bf16[2,16,256]{2,1,0:T(8,128)(2,1)S(1)} %fusion.45.bias_ref, f32[1,1024]{1,0:T(1,128)S(1)} %get-tuple-element.17.peak_ref, ...), custom_call_target="tpu_custom_call" | custom-call | flops 268435456 | bytes 327680 | tf_op jit(solution)/shard_map/fresh/pallas_call | solution.py:153
  148.3 4.2 %all-to-all-start.3 = ((bf16[8,72,128]{2,1,0:T(8,128)(2,1)}), bf16[8,72,128]{2,1,0:T(8,128)(2,1)}, u32[]{:S(2)}, u32[]{:S(2)}) async-start(bf16[8,72,128]{2,1,0:T(8,128)(2,1)} %fresh.2), calls=%async_computation.3 | async-start | bytes 294912 | tf_op jit(solution)/shard_map/all_to_all | solution.py:343
  152.5 18.8 %past.3 = (f32[1,1024]{1,0:T(1,128)S(1)}, f32[80,1024]{1,0:T(8,128)S(1)}) custom-call(bf16[8,136,128]{2,1,0:T(8,128)(2,1)S(1)} %all-to-all-done.1.q_ref, bf16[4,864,128]{2,1,0:T(8,128)(2,1)S(1)} %all-to-all-done.mine_ref, bf16[4,864,128]{2,1,0:T(8,128)(2,1)S(1)} %collective-permute-done.other_ref, bf16[4,16,768]{2,1,0:T(8,128)(2,1)S(1)} %reshape.384.mine_bias_ref, ...), custom_call_target="tpu_custom_call" | custom-call | flops 1610612736 | bytes 1769472 | tf_op jit(solution)/shard_map/past/pallas_call | solution.py:127
  171.3 4.1 %fresh.3 = bf16[8,72,128]{2,1,0:T(8,128)(2,1)} custom-call(s32[2]{0:T(128)S(1)} %add_multiply_fusion.place_ref, bf16[8,136,128]{2,1,0:T(8,128)(2,1)S(1)} %all-to-all-done.1.q_ref, bf16[2,256,128]{2,1,0:T(8,128)(2,1)S(1)} %bitcast.113, bf16[2,16,256]{2,1,0:T(8,128)(2,1)S(1)} %fusion.45.bias_ref, f32[1,1024]{1,0:T(1,128)S(1)} %get-tuple-element.20.peak_ref, ...), custom_call_target="tpu_custom_call" | custom-call | flops 268435456 | bytes 327680 | tf_op jit(solution)/shard_map/fresh/pallas_call | solution.py:153
  175.4 5.9 %all-to-all-done.3 = bf16[8,72,128]{2,1,0:T(8,128)(2,1)} async-done(((bf16[8,72,128]{2,1,0:T(8,128)(2,1)}), bf16[8,72,128]{2,1,0:T(8,128)(2,1)}, u32[]{:S(2)}, u32[]{:S(2)}) %all-to-all-start.3) | async-done | bytes 147488 | tf_op jit(solution)/shard_map/all_to_all | solution.py:343
  181.3 14.9 %all-to-all-start.4 = ((bf16[8,72,128]{2,1,0:T(8,128)(2,1)}), bf16[8,72,128]{2,1,0:T(8,128)(2,1)S(1)}, u32[]{:S(2)}, u32[]{:S(2)}) async-start(bf16[8,72,128]{2,1,0:T(8,128)(2,1)} %fresh.3), calls=%async_computation.4 | async-start | bytes 294912 | tf_op jit(solution)/shard_map/all_to_all | solution.py:343
  196.3 0.9 convert_element_type.99
  197.2 0.9 fusion.71
  198.1 25.9 %all-to-all-done.4 = bf16[8,72,128]{2,1,0:T(8,128)(2,1)S(1)} async-done(((bf16[8,72,128]{2,1,0:T(8,128)(2,1)}), bf16[8,72,128]{2,1,0:T(8,128)(2,1)S(1)}, u32[]{:S(2)}, u32[]{:S(2)}) %all-to-all-start.4) | async-done | bytes 147488 | tf_op jit(solution)/shard_map/all_to_all | solution.py:343
  225.2 9.0 %all_to_all.30 = bf16[4,66,256]{2,1,0:T(8,128)(2,1)S(1)} all-to-all(bf16[4,66,256]{2,1,0:T(8,128)(2,1)S(1)} %broadcast_in_dim.56), channel_id=1, replica_groups=mesh['grp'=2,'run'=8,'near'=4,'core'=2,'tp'=4] {'tp'}, dimensions={0} | all-to-all | bytes 270336 | tf_op jit(solution)/shard_map/all_to_all | solution.py:18
  (143 shorter events, 11.0 us)
Async XLA Ops:
  0.6 233.7 %copy-start = (bf16[1024,512]{1,0:T(8,128)(2,1)S(1)}, bf16[1024,512]{1,0:T(8,128)(2,1)}, u32[]{:S(2)}) copy-start(bf16[1024,512]{1,0:T(8,128)(2,1)} %param.29) | copy-start | bytes 3145732
  1.5 11.3 %copy-start.5 = (bf16[64,2048]{1,0:T(8,128)(2,1)S(1)}, bf16[64,2048]{1,0:T(8,128)(2,1)}, u32[]{:S(2)}) copy-start(bf16[64,2048]{1,0:T(8,128)(2,1)} %param.15) | copy-start | bytes 786436
  1.5 11.3 %copy-start.8 = (bf16[2,2048]{1,0:T(2,128)(2,1)S(1)}, bf16[2,2048]{1,0:T(2,128)(2,1)}, u32[]{:S(2)}) copy-start(bf16[2,2048]{1,0:T(2,128)(2,1)} %param.16) | copy-start | bytes 24580
  2.5 10.4 %copy-start.13 = (bf16[2048,4]{0,1:T(4,128)(2,1)S(1)}, bf16[2048,4]{0,1:T(4,128)(2,1)}, u32[]{:S(2)}) copy-start(bf16[2048,4]{0,1:T(4,128)(2,1)} %param.21) | copy-start | bytes 49156
  2.6 10.4 %copy-start.14 = (f32[2048]{0:T(1024)S(1)}, f32[2048]{0:T(1024)}, u32[]{:S(2)}) copy-start(f32[2048]{0:T(1024)} %param.17) | copy-start | bytes 24580
  2.6 10.4 %copy-start.15 = (f32[4]{0:T(128)S(1)}, f32[4]{0:T(128)}, u32[]{:S(2)}) copy-start(f32[4]{0:T(128)} %param.22) | copy-start | bytes 52
  3.6 9.7 %copy-start.9 = (f32[4,64]{1,0:T(4,128)S(1)}, f32[4,64]{1,0:T(4,128)}, u32[]{:S(2)}) copy-start(f32[4,64]{1,0:T(4,128)} %param.23) | copy-start | bytes 3076
  3.6 10.4 %copy-start.10 = (s32[2]{0:T(128)S(1)}, s32[2]{0:T(128)}, u32[]{:S(2)}) copy-start(s32[2]{0:T(128)} %param.28) | copy-start | bytes 28
  3.6 10.5 %copy-start.4 = (f32[2,4,3072]{2,1,0:T(4,128)S(1)}, f32[2,4,3072]{2,1,0:T(4,128)}, u32[]{:S(2)}) copy-start(f32[2,4,3072]{2,1,0:T(4,128)} %param.27) | copy-start | bytes 294916
  3.6 10.7 %copy-start.11 = (bf16[2048,64]{0,1:T(8,128)(2,1)S(1)}, bf16[2048,64]{0,1:T(8,128)(2,1)}, u32[]{:S(2)}) copy-start(bf16[2048,64]{0,1:T(8,128)(2,1)} %param.19) | copy-start | bytes 786436
  3.6 22.2 %all-to-all-start = ((bf16[4,864,128]{2,1,0:T(8,128)(2,1)}), bf16[4,864,128]{2,1,0:T(8,128)(2,1)S(1)}, u32[]{:S(2)}, u32[]{:S(2)}) async-start(bf16[4,864,128]{2,1,0:T(8,128)(2,1)} %broadcast_in_dim.47), calls=%async_computation | async-start | bytes 1769472 | tf_op jit(solution)/shard_map/all_to_all | solution.py:18
  12.8 1.8 copy-start.12
  14.6 2.7 %copy-start.6 = (bf16[66,64]{1,0:T(8,128)(2,1)}, bf16[66,64]{1,0:T(8,128)(2,1)S(1)}, u32[]{:S(2)}) copy-start(bf16[66,64]{1,0:T(8,128)(2,1)S(1)} %convolution_convert_fusion.3) | copy-start | bytes 25348
  14.9 63.7 %copy-start.7 = (bf16[66,64]{1,0:T(8,128)(2,1)}, bf16[66,64]{1,0:T(8,128)(2,1)S(1)}, u32[]{:S(2)}) copy-start(bf16[66,64]{1,0:T(8,128)(2,1)S(1)} %convolution_convert_fusion.2) | copy-start | bytes 25348
  26.5 81.4 %all-to-all-start.1 = ((bf16[8,136,128]{2,1,0:T(8,128)(2,1)}), bf16[8,136,128]{2,1,0:T(8,128)(2,1)S(1)}, u32[]{:S(2)}, u32[]{:S(2)}) async-start(bf16[8,136,128]{2,1,0:T(8,128)(2,1)} %broadcast_in_dim.48), calls=%async_computation.1 | async-start | bytes 557056 | tf_op jit(solution)/shard_map/all_to_all | solution.py:18
  75.9 32.4 %slice-start = ((bf16[66,64]{1,0:T(8,128)(2,1)}), bf16[64,64]{1,0:T(8,128)(2,1)S(1)}, s32[]{:S(2)}) async-start(bf16[66,64]{1,0:T(8,128)(2,1)} %copy-done.6), calls=%async_computation.6 | async-start | bytes 32768 | tf_op jit(solution)/shard_map/slice | solution.py:303
  78.7 29.6 %slice-start.1 = ((bf16[66,64]{1,0:T(8,128)(2,1)}), bf16[64,64]{1,0:T(8,128)(2,1)S(1)}, s32[]{:S(2)}) async-start(bf16[66,64]{1,0:T(8,128)(2,1)} %copy-done.7), calls=%async_computation.7 | async-start | bytes 32768 | tf_op jit(solution)/shard_map/slice | solution.py:303
  80.7 41.1 %collective-permute-start = (bf16[4,864,128]{2,1,0:T(8,128)(2,1)S(1)}, bf16[4,864,128]{2,1,0:T(8,128)(2,1)S(1)}, u32[]{:S(2)}, u32[]{:S(2)}) collective-permute-start(bf16[4,864,128]{2,1,0:T(8,128)(2,1)S(1)} %all-to-all-done.mine_ref), channel_id=1, source_target_pairs={{0,4},{4,0},{1,5},{5,1},{2,6},{6,2},{3,7},{7,3},{8,12},{12,8},{9,1... | collective-permute-start | bytes 2654216 | tf_op jit(solution)/shard_map/ppermute | solution.py:292
  109.0 32.5 %all-to-all-start.2 = ((bf16[8,72,128]{2,1,0:T(8,128)(2,1)}), bf16[8,72,128]{2,1,0:T(8,128)(2,1)S(1)}, u32[]{:S(2)}, u32[]{:S(2)}) async-start(bf16[8,72,128]{2,1,0:T(8,128)(2,1)} %broadcast_in_dim.55), calls=%async_computation.2 | async-start | bytes 294912 | tf_op jit(solution)/shard_map/all_to_all | solution.py:18
  140.8 0.7 copy-start.1
  141.5 0.7 copy-start.3
  143.2 1.0 copy-start.2
  148.3 33.0 %all-to-all-start.3 = ((bf16[8,72,128]{2,1,0:T(8,128)(2,1)}), bf16[8,72,128]{2,1,0:T(8,128)(2,1)}, u32[]{:S(2)}, u32[]{:S(2)}) async-start(bf16[8,72,128]{2,1,0:T(8,128)(2,1)} %fresh.2), calls=%async_computation.3 | async-start | bytes 294912 | tf_op jit(solution)/shard_map/all_to_all | solution.py:343
  181.3 42.7 %all-to-all-start.4 = ((bf16[8,72,128]{2,1,0:T(8,128)(2,1)}), bf16[8,72,128]{2,1,0:T(8,128)(2,1)S(1)}, u32[]{:S(2)}, u32[]{:S(2)}) async-start(bf16[8,72,128]{2,1,0:T(8,128)(2,1)} %fresh.3), calls=%async_computation.4 | async-start | bytes 294912 | tf_op jit(solution)/shard_map/all_to_all | solution.py:343

commit v3 on v2

--- a/solution.py
+++ b/solution.py
@@ -287,8 +287,7 @@
         ],
         axis=0,
     )
-    asked, mine = lax.optimization_barrier((asked, mine))
-    queries = to_each(asked, "run")
+    queries = lax.all_gather(asked, "run")
     other = lax.ppermute(mine, "core", [(0, 1), (1, 0)])
     mine_bias, other_bias = (
         block[:, past_rows:].reshape(-1, *past_bias.shape) for block in (mine, other)
@@ -307,16 +306,7 @@
         axis=0,
     )
     own = jnp.pad(own, ((0, -own.shape[0] % SPARE), (0, 0)))
-    dec_attn = decode_attention(
-        query[piece_count:].reshape(dec_count, pairs_here, group_size, head_width),
-        new_key[piece_count:].reshape(dec_count, pairs_here, head_width),
-        new_value[piece_count:].reshape(dec_count, pairs_here, head_width),
-        log_gate[piece_count:],
-        dec_cache,
-        dec_gate,
-        dec_lengths,
-    )
-    own, dec_attn = lax.optimization_barrier((own, dec_attn))
+    own, _ = lax.optimization_barrier((own, mine))
     news = to_each(own, ("near", "core"))
     run_rows = PIECES * heads_here * piece_count // width
     ran = news[:, piece_count : piece_count + run_rows].astype(jnp.float32)
@@ -334,13 +324,22 @@
     places = jnp.stack([me, run * neighbours]).astype(jnp.int32) * piece_count
 
     backs = []
-    asking = queries
+    asking, dec_query = queries, query[piece_count:]
     for side in range(2):
         sent = attend(
             side, places, asking, mine, other, mine_bias, other_bias, fresh, fresh_bias, past_rows, heads_here
         )
-        asking, sent, backs = lax.optimization_barrier((asking, sent, backs))
+        asking, sent, backs, dec_query = lax.optimization_barrier((asking, sent, backs, dec_query))
         backs = [*backs, lax.all_to_all(sent, "run", 0, 0, tiled=True)]
+    dec_attn = decode_attention(
+        dec_query.reshape(dec_count, pairs_here, group_size, head_width),
+        new_key[piece_count:].reshape(dec_count, pairs_here, head_width),
+        new_value[piece_count:].reshape(dec_count, pairs_here, head_width),
+        log_gate[piece_count:],
+        dec_cache,
+        dec_gate,
+        dec_lengths,
+    )
     columns = []
     for back in backs:
         part = merged(back, head_width).reshape(head_width, heads_here // 2, piece_count)

time: 240 us -> 242 us (level)
  blocking collectives: 9.02 us -> 82.4 us
  waiting for transfers between devices: 63.8 us -> 26.1 us
  starting transfers between devices: 93.7 us -> 56.8 us
    all_gather x0 -> x1, blocking collectives: none -> 73.4 us  [step(): queries = lax.all_gather(asked, 'run')]
    all_to_all x3 -> x2, starting transfers between devices: 71 us -> 25.5 us  [to_each(): lax.all_to_all(jnp.broadcast_to(array[None], (members, *array.shape)), ax...]
    all_to_all x3 -> x2, waiting for transfers between devices: 32 us -> 0.01 us  [to_each(): lax.all_to_all(jnp.broadcast_to(array[None], (members, *array.shape)), ax...]
    all_to_all x2, starting transfers between devices: 19.1 us -> 29.4 us  [step(): backs = [*backs, lax.all_to_all(sent, 'run', 0, 0, tiled=True)]]
    all_to_all x2, waiting for transfers between devices: 31.8 us -> 25.4 us  [step(): backs = [*backs, lax.all_to_all(sent, 'run', 0, 0, tiled=True)]]
  transfers between devices with their start and end apart: 6 -> 5, of which waited for: 4 -> 3; matrix products, arithmetic and copies ran while one was open for 5% -> 6% of each run, Pallas kernels for 18% -> 18%
where the time goes in v3:
time: 242 us; the launch traced here: 237 us
  blocking collectives  82.4 us (34%)
  starting transfers between devices  56.8 us (23%)
  Pallas kernels  45.9 us (19%)
  waiting for transfers between devices  26.1 us (11%)
  local copies, waits for them, and re-layouts  12.1 us (5%)
  other arithmetic  6.58 us (3%)
  matrix products  6.19 us (3%)
    all_gather x1, blocking collectives, step(): queries = lax.all_gather(asked, 'run')  73.4 us
    pallas_call x2, Pallas kernels, attend(): pl.pallas_call(functools.partial(past_kernel, first_head, heads), grid=(m...  37.7 us
    all_to_all x2, starting transfers between devices, step(): backs = [*backs, lax.all_to_all(sent, 'run', 0, 0, tiled=True)]  29.4 us
    all_to_all x2, starting transfers between devices, to_each(): lax.all_to_all(jnp.broadcast_to(array[None], (members, *array.shape)), ax...  25.5 us
    all_to_all x2, waiting for transfers between devices, step(): backs = [*backs, lax.all_to_all(sent, 'run', 0, 0, tiled=True)]  25.4 us
    all_to_all x1, blocking collectives, to_each(): lax.all_to_all(jnp.broadcast_to(array[None], (members, *array.shape)), ax...  9.04 us
    pallas_call x2, Pallas kernels, attend(): pl.pallas_call(functools.partial(fresh_kernel, first_head, heads), grid=(...  8.21 us
  transfers between devices with their start and end apart: 5, of which 3 were waited for; matrix products, arithmetic and copies ran while one was open for 6% of the time, Pallas kernels for 18%

profile of v3, /device:TPU:33, one launch (start us, length us, event | category | flops | bytes accessed | tf_op | source)
XLA Modules:
  0.0 237.3 jit_solution(6829406145047335861)
XLA Ops:
  0.6 0.8 reduce-precision_convert_fusion.1
  1.6 1.0 pad_maximum_fusion.1
  2.6 1.0 broadcast_in_dim.43
  3.6 9.2 %all-to-all-start = ((bf16[4,864,128]{2,1,0:T(8,128)(2,1)}), bf16[4,864,128]{2,1,0:T(8,128)(2,1)S(1)}, u32[]{:S(2)}, u32[]{:S(2)}) async-start(bf16[4,864,128]{2,1,0:T(8,128)(2,1)} %broadcast_in_dim.43), calls=%async_computation | async-start | bytes 1769472 | tf_op jit(solution)/shard_map/all_to_all | solution.py:18
  14.9 1.6 convolution_convert_fusion.1
  17.2 73.4 %all-gather = bf16[1088,128]{1,0:T(8,128)(2,1)S(1)} all-gather(bf16[136,128]{1,0:T(8,128)(2,1)S(1)} %maximum_maximum_fusion), channel_id=2, replica_groups=mesh['grp'=2,'run'=8,'near'=4,'core'=2,'tp'=4] {'run'}, dimensions={0}, use_global_device_ids=true | all-gather | bytes 313344 | tf_op jit(solution)/shard_map/all_gather | solution.py:290
  91.7 16.4 %all-to-all-start.1 = ((bf16[8,72,128]{2,1,0:T(8,128)(2,1)}), bf16[8,72,128]{2,1,0:T(8,128)(2,1)S(1)}, u32[]{:S(2)}, u32[]{:S(2)}) async-start(bf16[8,72,128]{2,1,0:T(8,128)(2,1)} %broadcast_in_dim.48), calls=%async_computation.1 | async-start | bytes 294912 | tf_op jit(solution)/shard_map/all_to_all | solution.py:18
  108.1 1.9 collective-permute-start
  112.5 18.8 %past.2 = (f32[1,1024]{1,0:T(1,128)S(1)}, f32[80,1024]{1,0:T(8,128)S(1)}) custom-call(bf16[8,136,128]{2,1,0:T(8,128)(2,1)S(1)} %bitcast.110, bf16[4,864,128]{2,1,0:T(8,128)(2,1)S(1)} %all-to-all-done.mine_ref, bf16[4,864,128]{2,1,0:T(8,128)(2,1)S(1)} %collective-permute-done.other_ref, bf16[4,16,768]{2,1,0:T(8,128)(2,1)S(1)} %reshape.381.mine_bias_ref, ...), custom_call_target="tpu_custom_call" | custom-call | flops 1610612736 | bytes 1769472 | tf_op jit(solution)/shard_map/past/pallas_call | solution.py:127
  132.9 0.9 slice.140
  133.8 1.0 copy-done.2
  134.8 4.1 %fresh.2 = bf16[8,72,128]{2,1,0:T(8,128)(2,1)} custom-call(s32[2]{0:T(128)S(1)} %add_multiply_fusion.place_ref, bf16[8,136,128]{2,1,0:T(8,128)(2,1)S(1)} %bitcast.111, bf16[2,256,128]{2,1,0:T(8,128)(2,1)S(1)} %bitcast.114, bf16[2,16,256]{2,1,0:T(8,128)(2,1)S(1)} %fusion.45.bias_ref, f32[1,1024]{1,0:T(1,128)S(1)} %get-tuple-element.14.peak_ref, ...), custom_call_target="tpu_custom_call" | custom-call | flops 268435456 | bytes 327680 | tf_op jit(solution)/shard_map/fresh/pallas_call | solution.py:153
  138.9 11.2 %all-to-all-start.2 = ((bf16[8,72,128]{2,1,0:T(8,128)(2,1)}), bf16[8,72,128]{2,1,0:T(8,128)(2,1)}, u32[]{:S(2)}, u32[]{:S(2)}) async-start(bf16[8,72,128]{2,1,0:T(8,128)(2,1)} %fresh.2), calls=%async_computation.2 | async-start | bytes 294912 | tf_op jit(solution)/shard_map/all_to_all | solution.py:333
  150.1 1.2 slice_bitcast_fusion
  151.3 1.3 iota_compare_fusion.4
  152.7 18.8 %past.3 = (f32[1,1024]{1,0:T(1,128)S(1)}, f32[80,1024]{1,0:T(8,128)S(1)}) custom-call(bf16[8,136,128]{2,1,0:T(8,128)(2,1)S(1)} %bitcast.112, bf16[4,864,128]{2,1,0:T(8,128)(2,1)S(1)} %all-to-all-done.mine_ref, bf16[4,864,128]{2,1,0:T(8,128)(2,1)S(1)} %collective-permute-done.other_ref, bf16[4,16,768]{2,1,0:T(8,128)(2,1)S(1)} %reshape.381.mine_bias_ref, ...), custom_call_target="tpu_custom_call" | custom-call | flops 1610612736 | bytes 1769472 | tf_op jit(solution)/shard_map/past/pallas_call | solution.py:127
  171.5 4.1 %fresh.3 = bf16[8,72,128]{2,1,0:T(8,128)(2,1)} custom-call(s32[2]{0:T(128)S(1)} %add_multiply_fusion.place_ref, bf16[8,136,128]{2,1,0:T(8,128)(2,1)S(1)} %bitcast.113, bf16[2,256,128]{2,1,0:T(8,128)(2,1)S(1)} %bitcast.115, bf16[2,16,256]{2,1,0:T(8,128)(2,1)S(1)} %fusion.45.bias_ref, f32[1,1024]{1,0:T(1,128)S(1)} %get-tuple-element.17.peak_ref, ...), custom_call_target="tpu_custom_call" | custom-call | flops 268435456 | bytes 327680 | tf_op jit(solution)/shard_map/fresh/pallas_call | solution.py:153
  175.6 3.0 %all-to-all-done.2 = bf16[8,72,128]{2,1,0:T(8,128)(2,1)} async-done(((bf16[8,72,128]{2,1,0:T(8,128)(2,1)}), bf16[8,72,128]{2,1,0:T(8,128)(2,1)}, u32[]{:S(2)}, u32[]{:S(2)}) %all-to-all-start.2) | async-done | bytes 147488 | tf_op jit(solution)/shard_map/all_to_all | solution.py:333
  179.6 18.2 %all-to-all-start.3 = ((bf16[8,72,128]{2,1,0:T(8,128)(2,1)}), bf16[8,72,128]{2,1,0:T(8,128)(2,1)S(1)}, u32[]{:S(2)}, u32[]{:S(2)}) async-start(bf16[8,72,128]{2,1,0:T(8,128)(2,1)} %fresh.3), calls=%async_computation.3 | async-start | bytes 294912 | tf_op jit(solution)/shard_map/all_to_all | solution.py:333
  197.8 2.0 fusion.73
  201.3 0.9 convert_element_type.95
  202.2 0.9 fusion.71
  203.1 22.3 %all-to-all-done.3 = bf16[8,72,128]{2,1,0:T(8,128)(2,1)S(1)} async-done(((bf16[8,72,128]{2,1,0:T(8,128)(2,1)}), bf16[8,72,128]{2,1,0:T(8,128)(2,1)S(1)}, u32[]{:S(2)}, u32[]{:S(2)}) %all-to-all-start.3) | async-done | bytes 147488 | tf_op jit(solution)/shard_map/all_to_all | solution.py:333
  226.6 9.0 %all_to_all.25 = bf16[4,66,256]{2,1,0:T(8,128)(2,1)S(1)} all-to-all(bf16[4,66,256]{2,1,0:T(8,128)(2,1)S(1)} %broadcast_in_dim.53), channel_id=1, replica_groups=mesh['grp'=2,'run'=8,'near'=4,'core'=2,'tp'=4] {'tp'}, dimensions={0} | all-to-all | bytes 270336 | tf_op jit(solution)/shard_map/all_to_all | solution.py:18
  (148 shorter events, 12.9 us)
Async XLA Ops:
  0.6 235.1 %copy-start = (bf16[1024,512]{1,0:T(8,128)(2,1)S(1)}, bf16[1024,512]{1,0:T(8,128)(2,1)}, u32[]{:S(2)}) copy-start(bf16[1024,512]{1,0:T(8,128)(2,1)} %param.29) | copy-start | bytes 3145732
  1.5 11.3 %copy-start.7 = (bf16[64,2048]{1,0:T(8,128)(2,1)S(1)}, bf16[64,2048]{1,0:T(8,128)(2,1)}, u32[]{:S(2)}) copy-start(bf16[64,2048]{1,0:T(8,128)(2,1)} %param.15) | copy-start | bytes 786436
  1.5 11.2 %copy-start.10 = (bf16[2,2048]{1,0:T(2,128)(2,1)S(1)}, bf16[2,2048]{1,0:T(2,128)(2,1)}, u32[]{:S(2)}) copy-start(bf16[2,2048]{1,0:T(2,128)(2,1)} %param.16) | copy-start | bytes 24580
  2.5 10.4 %copy-start.16 = (bf16[2048,4]{0,1:T(4,128)(2,1)S(1)}, bf16[2048,4]{0,1:T(4,128)(2,1)}, u32[]{:S(2)}) copy-start(bf16[2048,4]{0,1:T(4,128)(2,1)} %param.21) | copy-start | bytes 49156
  2.6 10.4 %copy-start.17 = (f32[2048]{0:T(1024)S(1)}, f32[2048]{0:T(1024)}, u32[]{:S(2)}) copy-start(f32[2048]{0:T(1024)} %param.17) | copy-start | bytes 24580
  2.6 10.4 %copy-start.18 = (f32[4]{0:T(128)S(1)}, f32[4]{0:T(128)}, u32[]{:S(2)}) copy-start(f32[4]{0:T(128)} %param.22) | copy-start | bytes 52
  3.6 9.7 %copy-start.12 = (f32[4,64]{1,0:T(4,128)S(1)}, f32[4,64]{1,0:T(4,128)}, u32[]{:S(2)}) copy-start(f32[4,64]{1,0:T(4,128)} %param.23) | copy-start | bytes 3076
  3.6 10.3 %copy-start.14 = (bf16[2048,64]{0,1:T(8,128)(2,1)S(1)}, bf16[2048,64]{0,1:T(8,128)(2,1)}, u32[]{:S(2)}) copy-start(bf16[2048,64]{0,1:T(8,128)(2,1)} %param.19) | copy-start | bytes 786436
  3.6 10.7 %copy-start.15 = (bf16[2048,64]{0,1:T(8,128)(2,1)S(1)}, bf16[2048,64]{0,1:T(8,128)(2,1)}, u32[]{:S(2)}) copy-start(bf16[2048,64]{0,1:T(8,128)(2,1)} %param.20) | copy-start | bytes 786436
  3.6 87.4 %all-to-all-start = ((bf16[4,864,128]{2,1,0:T(8,128)(2,1)}), bf16[4,864,128]{2,1,0:T(8,128)(2,1)S(1)}, u32[]{:S(2)}, u32[]{:S(2)}) async-start(bf16[4,864,128]{2,1,0:T(8,128)(2,1)} %broadcast_in_dim.43), calls=%async_computation | async-start | bytes 1769472 | tf_op jit(solution)/shard_map/all_to_all | solution.py:18
  14.3 76.7 %copy-start.13 = (s32[2]{0:T(128)S(1)}, s32[2]{0:T(128)}, u32[]{:S(2)}) copy-start(s32[2]{0:T(128)} %param.28) | copy-start | bytes 28
  14.9 95.2 %copy-start.5 = (f32[2,4,3072]{2,1,0:T(4,128)S(1)}, f32[2,4,3072]{2,1,0:T(4,128)}, u32[]{:S(2)}) copy-start(f32[2,4,3072]{2,1,0:T(4,128)} %param.27) | copy-start | bytes 294916
  91.7 40.4 %all-to-all-start.1 = ((bf16[8,72,128]{2,1,0:T(8,128)(2,1)}), bf16[8,72,128]{2,1,0:T(8,128)(2,1)S(1)}, u32[]{:S(2)}, u32[]{:S(2)}) async-start(bf16[8,72,128]{2,1,0:T(8,128)(2,1)} %broadcast_in_dim.48), calls=%async_computation.1 | async-start | bytes 294912 | tf_op jit(solution)/shard_map/all_to_all | solution.py:18
  108.1 4.3 %collective-permute-start = (bf16[4,864,128]{2,1,0:T(8,128)(2,1)S(1)}, bf16[4,864,128]{2,1,0:T(8,128)(2,1)S(1)}, u32[]{:S(2)}, u32[]{:S(2)}) collective-permute-start(bf16[4,864,128]{2,1,0:T(8,128)(2,1)S(1)} %all-to-all-done.mine_ref), channel_id=1, source_target_pairs={{0,4},{4,0},{1,5},{5,1},{2,6},{6,2},{3,7},{7,3},{8,12},{12,8},{9,1... | collective-permute-start | bytes 2654216 | tf_op jit(solution)/shard_map/ppermute | solution.py:291
  131.4 0.7 copy-start.1
  132.1 0.7 copy-start.4
  133.8 1.0 copy-start.2
  138.9 39.8 %all-to-all-start.2 = ((bf16[8,72,128]{2,1,0:T(8,128)(2,1)}), bf16[8,72,128]{2,1,0:T(8,128)(2,1)}, u32[]{:S(2)}, u32[]{:S(2)}) async-start(bf16[8,72,128]{2,1,0:T(8,128)(2,1)} %fresh.2), calls=%async_computation.2 | async-start | bytes 294912 | tf_op jit(solution)/shard_map/all_to_all | solution.py:333
  152.7 26.0 %slice-start = ((bf16[66,256]{1,0:T(8,128)(2,1)}), bf16[2,256]{1,0:T(2,128)(2,1)S(1)}, s32[]{:S(2)}) async-start(bf16[66,256]{1,0:T(8,128)(2,1)} %copy-done.8), calls=%async_computation.5 | async-start | bytes 2048 | tf_op jit(solution)/shard_map/slice | solution.py:327
  152.7 45.1 %copy-start.6 = (f32[2,4,3072]{2,1,0:T(4,128)S(1)}, f32[2,4,3072]{2,1,0:T(4,128)}, u32[]{:S(2)}) copy-start(f32[2,4,3072]{2,1,0:T(4,128)} %param.27) | copy-start | bytes 294916
  171.5 28.4 %copy-start.11 = (f32[2,4]{0,1:T(4,128)S(1)}, f32[2,4]{0,1:T(4,128)}, u32[]{:S(2)}) copy-start(f32[2,4]{0,1:T(4,128)} %copy.118) | copy-start | bytes 100
  171.5 29.1 %copy-start.19 = (f32[2,64]{1,0:T(2,128)S(1)}, f32[2,64]{1,0:T(2,128)}, u32[]{:S(2)}) copy-start(f32[2,64]{1,0:T(2,128)} %slice_convert_fusion.3) | copy-start | bytes 1540
  175.6 25.0 %copy-start.3 = (bf16[2,3072,1,128]{3,1,2,0:T(8,128)(2,1)S(1)}, bf16[2,3072,1,128]{3,1,2,0:T(8,128)(2,1)}, u32[]{:S(2)}) copy-start(bf16[2,3072,1,128]{3,1,2,0:T(8,128)(2,1)} %param.26) | copy-start | bytes 4718596
  179.6 45.8 %all-to-all-start.3 = ((bf16[8,72,128]{2,1,0:T(8,128)(2,1)}), bf16[8,72,128]{2,1,0:T(8,128)(2,1)S(1)}, u32[]{:S(2)}, u32[]{:S(2)}) async-start(bf16[8,72,128]{2,1,0:T(8,128)(2,1)} %fresh.3), calls=%async_computation.3 | async-start | bytes 294912 | tf_op jit(solution)/shard_map/all_to_all | solution.py:333
  (2 other events, 1.2 us)

commit v4 on v3

--- a/solution.py
+++ b/solution.py
@@ -11,6 +11,8 @@
 GRP_KV = ("grp", "run", "near", "core")
 PIECES = 3
 SPARE = 8
+AT_ONCE = 4
+JOINED = 4
 
 
 def to_each(array, axis):
@@ -59,19 +61,19 @@
     return [first, second, left - second]
 
 
-def query_tile(q_ref, first_head, heads):
+def query_tile(q_ref, heads):
     members, width, lanes = q_ref.shape
     turned = jnp.concatenate([q_ref[k] for k in range(members)], axis=1)
-    each = lanes // (heads // 2)
+    each = lanes // heads
     shape = (width, members * lanes)
     row = lax.broadcasted_iota(jnp.int32, shape, 0)
-    head = first_head + lax.broadcasted_iota(jnp.int32, shape, 1) % lanes // each
+    head = lax.broadcasted_iota(jnp.int32, shape, 1) % lanes // each
     pick = (row % heads == head) & (row < PIECES * heads)
     return jnp.concatenate([turned, pick.astype(jnp.float32).astype(jnp.bfloat16)], axis=0)
 
 
-def past_kernel(first_head, heads, q_ref, mine_ref, other_ref, mine_bias_ref, other_bias_ref, peak_ref, acc_ref):
-    query = query_tile(q_ref, first_head, heads)
+def past_kernel(heads, q_ref, mine_ref, other_ref, mine_bias_ref, other_bias_ref, peak_ref, acc_ref):
+    query = query_tile(q_ref, heads)
 
     @pl.when(pl.program_id(1) == 0)
     def _():
@@ -87,12 +89,12 @@
     peak_ref[...], acc_ref[...] = state
 
 
-def fresh_kernel(first_head, heads, place_ref, q_ref, kv_ref, bias_ref, peak_ref, acc_ref, out_ref):
-    query = query_tile(q_ref, first_head, heads)
+def fresh_kernel(heads, place_ref, q_ref, kv_ref, bias_ref, peak_ref, acc_ref, out_ref):
+    query = query_tile(q_ref, heads)
     width, tile = query.shape
     half = width // 2
     members, _, lanes = out_ref.shape
-    each = lanes // (heads // 2)
+    each = lanes // heads
     chunks, count, _ = kv_ref.shape
     state = peak_ref[...], acc_ref[...]
     lane = lax.broadcasted_iota(jnp.int32, (1, tile), 1)
@@ -112,23 +114,22 @@
         out_ref[k] = sent[:, k * lanes : (k + 1) * lanes]
 
 
-def attend(side, places, queries, mine, other, mine_bias, other_bias, fresh, fresh_bias, past_rows, heads):
+def attend(places, queries, mine, other, mine_bias, other_bias, fresh, fresh_bias, past_rows, heads):
     members, _, lanes = queries.shape
     shards, _, width = mine.shape
     half = width // 2
-    at_once, joined = 2, 2
+    at_once, joined = AT_ONCE, JOINED
     tile = joined * lanes
     rows = members * lanes
     whole = lambda array: pl.BlockSpec(array.shape, lambda *_: (0,) * array.ndim)
     shard = lambda count: pl.BlockSpec((at_once, count, width), lambda r, s: (s, 0, 0))
     bias_block = pl.BlockSpec((at_once, *mine_bias.shape[1:]), lambda r, s: (s, 0, 0))
-    first_head = side * (heads // 2)
     work = 2 * shards * past_rows * rows
     peak, acc = pl.pallas_call(
-        functools.partial(past_kernel, first_head, heads),
+        functools.partial(past_kernel, heads),
         grid=(members // joined, shards // at_once),
         in_specs=[
-            pl.BlockSpec((joined, half, lanes), lambda r, s: (r, side, 0)),
+            pl.BlockSpec((joined, half, lanes), lambda r, s: (r, 0, 0)),
             shard(past_rows),
             shard(past_rows),
             bias_block,
@@ -151,11 +152,11 @@
         name="past",
     )(queries, mine, other, mine_bias, other_bias)
     return pl.pallas_call(
-        functools.partial(fresh_kernel, first_head, heads),
+        functools.partial(fresh_kernel, heads),
         grid=(members // joined,),
         in_specs=[
             pl.BlockSpec(memory_space=pltpu.SMEM),
-            pl.BlockSpec((joined, half, lanes), lambda r: (r, side, 0)),
+            pl.BlockSpec((joined, half, lanes), lambda r: (r, 0, 0)),
             whole(fresh),
             whole(fresh_bias),
             pl.BlockSpec((1, tile), lambda r: (0, r)),
@@ -259,7 +260,7 @@
     head_width = width // 2
     heads_here = w_forget.shape[1]
     group_size = heads_here // pairs_here
-    lanes = heads_here // 2 * piece_count
+    lanes = heads_here * piece_count
     neighbours = lax.axis_size(("near", "core"))
     me = lax.axis_index(("near", "core"))
     run = lax.axis_index("run")
@@ -278,10 +279,10 @@
     running = jnp.cumsum(log_gate[:piece_count].T + piece_decay, axis=1)
 
     scaled = query[:piece_count] * jnp.asarray(head_width ** (-0.5), query.dtype)
-    turned = scaled.reshape(piece_count, 2, heads_here // 2, head_width).transpose(1, 3, 2, 0)
+    turned = scaled.reshape(piece_count, heads_here, head_width).transpose(2, 1, 0)
     asked = jnp.concatenate(
         [
-            turned.reshape(2 * head_width, lanes),
+            turned.reshape(head_width, lanes),
             packed(bf16_pieces(running[None, :, -1], 0), lanes),
             jnp.zeros((SPARE - 1, lanes), jnp.bfloat16),
         ],
@@ -292,7 +293,7 @@
     mine_bias, other_bias = (
         block[:, past_rows:].reshape(-1, *past_bias.shape) for block in (mine, other)
     )
-    totals = queries[:, 2 * head_width, : PIECES * heads_here].astype(jnp.float32)
+    totals = queries[:, head_width, : PIECES * heads_here].astype(jnp.float32)
     totals = totals.reshape(-1, PIECES, heads_here).sum(1)
     earlier = jnp.arange(totals.shape[0], dtype=jnp.int32)[:, None] < run
     earlier = jnp.sum(jnp.where(earlier, totals, 0.0), axis=0)
@@ -323,14 +324,11 @@
     fresh = news[:, :piece_count].reshape(chunks, joined * piece_count, width)
     places = jnp.stack([me, run * neighbours]).astype(jnp.int32) * piece_count
 
-    backs = []
-    asking, dec_query = queries, query[piece_count:]
-    for side in range(2):
-        sent = attend(
-            side, places, asking, mine, other, mine_bias, other_bias, fresh, fresh_bias, past_rows, heads_here
-        )
-        asking, sent, backs, dec_query = lax.optimization_barrier((asking, sent, backs, dec_query))
-        backs = [*backs, lax.all_to_all(sent, "run", 0, 0, tiled=True)]
+    sent = attend(
+        places, queries, mine, other, mine_bias, other_bias, fresh, fresh_bias, past_rows, heads_here
+    )
+    sent, dec_query = lax.optimization_barrier((sent, query[piece_count:]))
+    back = lax.all_to_all(sent, "run", 0, 0, tiled=True)
     dec_attn = decode_attention(
         dec_query.reshape(dec_count, pairs_here, group_size, head_width),
         new_key[piece_count:].reshape(dec_count, pairs_here, head_width),
@@ -340,12 +338,10 @@
         dec_gate,
         dec_lengths,
     )
-    columns = []
-    for back in backs:
-        part = merged(back, head_width).reshape(head_width, heads_here // 2, piece_count)
-        columns.append(part.transpose(2, 1, 0).reshape(piece_count, -1))
+    piece_attn = merged(back, head_width).reshape(head_width, heads_here, piece_count)
+    piece_attn = piece_attn.transpose(2, 1, 0).reshape(piece_count, -1)
     attn_rows = jnp.concatenate(
-        [jnp.concatenate(columns, axis=1), dec_attn.reshape(dec_count, heads_here * head_width)],
+        [piece_attn, dec_attn.reshape(dec_count, heads_here * head_width)],
         axis=0,
     ).astype(jnp.bfloat16)
     every_head = jnp.moveaxis(to_each(attn_rows, "tp"), 0, 1).reshape(attn_rows.shape[0], -1)

time: 242 us -> 207 us (0.86)
  the two profiles are of different devices: /device:TPU:33 before, /device:TPU:104 now
where the time goes in v4:
time: 207 us; the launch traced here: 206 us
  blocking collectives  95.3 us (46%)
  waiting for transfers between devices  39.9 us (19%)
  starting transfers between devices  25.5 us (12%)
  Pallas kernels  24.7 us (12%)
  local copies, waits for them, and re-layouts  9.57 us (5%)
  matrix products  6.17 us (3%)
  other arithmetic  3.74 us (2%)
    all_gather x1, blocking collectives, step(): queries = lax.all_gather(asked, 'run')  84.8 us
    all_to_all x1, waiting for transfers between devices, step(): back = lax.all_to_all(sent, 'run', 0, 0, tiled=True)  39.9 us
    pallas_call x1, Pallas kernels, attend(): pl.pallas_call(functools.partial(past_kernel, heads), grid=(members // jo...  20.9 us
    all_to_all x2, starting transfers between devices, to_each(): lax.all_to_all(jnp.broadcast_to(array[None], (members, *array.shape)), ax...  12.1 us
    all_to_all x1, starting transfers between devices, step(): back = lax.all_to_all(sent, 'run', 0, 0, tiled=True)  11.5 us
    all_to_all x1, blocking collectives, to_each(): lax.all_to_all(jnp.broadcast_to(array[None], (members, *array.shape)), ax...  10.5 us
  transfers between devices with their start and end apart: 4, of which 1 were waited for; matrix products, arithmetic and copies ran while one was open for 6% of the time, Pallas kernels for 10%

profile of v4, /device:TPU:104, one launch (start us, length us, event | category | flops | bytes accessed | tf_op | source)
XLA Modules:
  0.0 206.0 jit_solution(877775369114190982)
XLA Ops:
  0.6 0.8 reduce-precision_convert_fusion.1
  1.6 1.0 pad_maximum_fusion.1
  2.6 1.0 broadcast_in_dim.43
  3.6 7.9 %all-to-all-start = ((bf16[4,864,128]{2,1,0:T(8,128)(2,1)}), bf16[4,864,128]{2,1,0:T(8,128)(2,1)S(1)}, u32[]{:S(2)}, u32[]{:S(2)}) async-start(bf16[4,864,128]{2,1,0:T(8,128)(2,1)} %broadcast_in_dim.43), calls=%async_computation | async-start | bytes 1769472 | tf_op jit(solution)/shard_map/all_to_all | solution.py:20
  12.7 1.2 convolution_convert_fusion.3
  14.0 1.2 convolution_convert_fusion.2
  15.2 0.3 convolution_convert_fusion.1
  16.1 84.8 %all-gather = bf16[576,256]{1,0:T(8,128)(2,1)S(1)} all-gather(bf16[72,256]{1,0:T(8,128)(2,1)S(1)} %maximum_maximum_fusion), channel_id=2, replica_groups=mesh['grp'=2,'run'=8,'near'=4,'core'=2,'tp'=4] {'run'}, dimensions={0}, use_global_device_ids=true | all-gather | bytes 331776 | tf_op jit(solution)/shard_map/all_gather | solution.py:291
  101.3 2.0 collective-permute-start
  103.4 0.7 broadcast_in_dim.48
  104.1 4.2 %all-to-all-start.1 = ((bf16[8,72,128]{2,1,0:T(8,128)(2,1)}), bf16[8,72,128]{2,1,0:T(8,128)(2,1)S(1)}, u32[]{:S(2)}, u32[]{:S(2)}) async-start(bf16[8,72,128]{2,1,0:T(8,128)(2,1)} %broadcast_in_dim.48), calls=%async_computation.1 | async-start | bytes 294912 | tf_op jit(solution)/shard_map/all_to_all | solution.py:20
  108.6 0.6 slice.117
  109.2 1.0 reshape.359.other_bias_ref
  110.2 20.9 %past.1 = (f32[1,2048]{1,0:T(1,128)S(1)}, f32[80,2048]{1,0:T(8,128)S(1)}) custom-call(bf16[8,72,256]{2,1,0:T(8,128)(2,1)S(1)} %bitcast.90, bf16[4,864,128]{2,1,0:T(8,128)(2,1)S(1)} %all-to-all-done.mine_ref, bf16[4,864,128]{2,1,0:T(8,128)(2,1)S(1)} %collective-permute-done.other_ref, bf16[4,16,768]{2,1,0:T(8,128)(2,1)S(1)} %reshape.358.mine_bias_ref, ...), custom_call_target="tpu_custom_call" | custom-call | flops 3221225472 | bytes 1769472 | tf_op jit(solution)/shard_map/past/pallas_call | solution.py:128
  131.1 0.8 copy-done.1
  132.8 1.1 copy-done.2
  133.9 3.8 %fresh.1 = bf16[8,72,256]{2,1,0:T(8,128)(2,1)} custom-call(s32[2]{0:T(128)S(1)} %add_multiply_fusion.place_ref, bf16[8,72,256]{2,1,0:T(8,128)(2,1)S(1)} %bitcast.91, bf16[2,256,128]{2,1,0:T(8,128)(2,1)S(1)} %bitcast.92, bf16[2,16,256]{2,1,0:T(8,128)(2,1)S(1)} %fusion.43.bias_ref, f32[1,2048]{1,0:T(1,128)S(1)} %get-tuple-element.8.peak_ref, ...), custom_call_target="tpu_custom_call" | custom-call | flops 536870912 | bytes 655360 | tf_op jit(solution)/shard_map/fresh/pallas_call | solution.py:154
  137.6 11.5 %all-to-all-start.2 = ((bf16[8,72,256]{2,1,0:T(8,128)(2,1)}), bf16[8,72,256]{2,1,0:T(8,128)(2,1)S(1)}, u32[]{:S(2)}, u32[]{:S(2)}) async-start(bf16[8,72,256]{2,1,0:T(8,128)(2,1)} %fresh.1), calls=%async_computation.2 | async-start | bytes 589824 | tf_op jit(solution)/shard_map/all_to_all | solution.py:331
  149.7 2.0 fusion.65
  152.5 0.6 fusion.14
  153.2 39.9 %all-to-all-done.2 = bf16[8,72,256]{2,1,0:T(8,128)(2,1)S(1)} async-done(((bf16[8,72,256]{2,1,0:T(8,128)(2,1)}), bf16[8,72,256]{2,1,0:T(8,128)(2,1)S(1)}, u32[]{:S(2)}, u32[]{:S(2)}) %all-to-all-start.2) | async-done | bytes 294944 | tf_op jit(solution)/shard_map/all_to_all | solution.py:331
  193.8 10.5 %all_to_all.20 = bf16[4,66,256]{2,1,0:T(8,128)(2,1)S(1)} all-to-all(bf16[4,66,256]{2,1,0:T(8,128)(2,1)S(1)} %broadcast_in_dim.53), channel_id=1, replica_groups=mesh['grp'=2,'run'=8,'near'=4,'core'=2,'tp'=4] {'tp'}, dimensions={0} | all-to-all | bytes 270336 | tf_op jit(solution)/shard_map/all_to_all | solution.py:20
  204.8 0.6 slice.129
  205.4 0.6 slice.128
  (122 shorter events, 5.8 us)
Async XLA Ops:
  0.6 203.9 %copy-start = (bf16[1024,512]{1,0:T(8,128)(2,1)S(1)}, bf16[1024,512]{1,0:T(8,128)(2,1)}, u32[]{:S(2)}) copy-start(bf16[1024,512]{1,0:T(8,128)(2,1)} %param.29) | copy-start | bytes 3145732
  1.5 10.0 %copy-start.5 = (bf16[64,2048]{1,0:T(8,128)(2,1)S(1)}, bf16[64,2048]{1,0:T(8,128)(2,1)}, u32[]{:S(2)}) copy-start(bf16[64,2048]{1,0:T(8,128)(2,1)} %param.15) | copy-start | bytes 786436
  1.5 9.9 %copy-start.7 = (bf16[2,2048]{1,0:T(2,128)(2,1)S(1)}, bf16[2,2048]{1,0:T(2,128)(2,1)}, u32[]{:S(2)}) copy-start(bf16[2,2048]{1,0:T(2,128)(2,1)} %param.16) | copy-start | bytes 24580
  2.5 9.1 %copy-start.11 = (bf16[2048,4]{0,1:T(4,128)(2,1)S(1)}, bf16[2048,4]{0,1:T(4,128)(2,1)}, u32[]{:S(2)}) copy-start(bf16[2048,4]{0,1:T(4,128)(2,1)} %param.21) | copy-start | bytes 49156
  2.6 9.1 %copy-start.12 = (f32[2048]{0:T(1024)S(1)}, f32[2048]{0:T(1024)}, u32[]{:S(2)}) copy-start(f32[2048]{0:T(1024)} %param.17) | copy-start | bytes 24580
  2.6 9.1 %copy-start.13 = (f32[4]{0:T(128)S(1)}, f32[4]{0:T(128)}, u32[]{:S(2)}) copy-start(f32[4]{0:T(128)} %param.22) | copy-start | bytes 52
  3.6 8.4 %copy-start.8 = (f32[4,64]{1,0:T(4,128)S(1)}, f32[4,64]{1,0:T(4,128)}, u32[]{:S(2)}) copy-start(f32[4,64]{1,0:T(4,128)} %param.23) | copy-start | bytes 3076
  3.6 97.7 %all-to-all-start = ((bf16[4,864,128]{2,1,0:T(8,128)(2,1)}), bf16[4,864,128]{2,1,0:T(8,128)(2,1)S(1)}, u32[]{:S(2)}, u32[]{:S(2)}) async-start(bf16[4,864,128]{2,1,0:T(8,128)(2,1)} %broadcast_in_dim.43), calls=%async_computation | async-start | bytes 1769472 | tf_op jit(solution)/shard_map/all_to_all | solution.py:20
  11.7 3.6 %copy-start.10 = (bf16[2048,256]{1,0:T(8,128)(2,1)S(1)}, bf16[2048,256]{1,0:T(8,128)(2,1)}, u32[]{:S(2)}) copy-start(bf16[2048,256]{1,0:T(8,128)(2,1)} %param.18) | copy-start | bytes 3145732
  13.9 87.3 %copy-start.9 = (s32[2]{0:T(128)S(1)}, s32[2]{0:T(128)}, u32[]{:S(2)}) copy-start(s32[2]{0:T(128)} %param.28) | copy-start | bytes 28
  15.6 115.5 %copy-start.6 = (bf16[66,256]{1,0:T(8,128)(2,1)}, bf16[66,256]{1,0:T(8,128)(2,1)S(1)}, u32[]{:S(2)}) copy-start(bf16[66,256]{1,0:T(8,128)(2,1)S(1)} %convolution_convert_fusion.1) | copy-start | bytes 101380
  101.3 7.2 %collective-permute-start = (bf16[4,864,128]{2,1,0:T(8,128)(2,1)S(1)}, bf16[4,864,128]{2,1,0:T(8,128)(2,1)S(1)}, u32[]{:S(2)}, u32[]{:S(2)}) collective-permute-start(bf16[4,864,128]{2,1,0:T(8,128)(2,1)S(1)} %all-to-all-done.mine_ref), channel_id=1, source_target_pairs={{0,4},{4,0},{1,5},{5,1},{2,6},{6,2},{3,7},{7,3},{8,12},{12,8},{9,1... | collective-permute-start | bytes 2654216 | tf_op jit(solution)/shard_map/ppermute | solution.py:292
  104.1 27.9 %all-to-all-start.1 = ((bf16[8,72,128]{2,1,0:T(8,128)(2,1)}), bf16[8,72,128]{2,1,0:T(8,128)(2,1)S(1)}, u32[]{:S(2)}, u32[]{:S(2)}) async-start(bf16[8,72,128]{2,1,0:T(8,128)(2,1)} %broadcast_in_dim.48), calls=%async_computation.1 | async-start | bytes 294912 | tf_op jit(solution)/shard_map/all_to_all | solution.py:20
  131.1 0.8 copy-start.1
  132.2 16.9 %copy-start.4 = (f32[2,4,3072]{2,1,0:T(4,128)S(1)}, f32[2,4,3072]{2,1,0:T(4,128)}, u32[]{:S(2)}) copy-start(f32[2,4,3072]{2,1,0:T(4,128)} %param.27) | copy-start | bytes 294916
  132.3 17.2 %slice-start = ((bf16[66,256]{1,0:T(8,128)(2,1)}), bf16[2,256]{1,0:T(2,128)(2,1)S(1)}, s32[]{:S(2)}) async-start(bf16[66,256]{1,0:T(8,128)(2,1)} %copy-done.6), calls=%async_computation.4 | async-start | bytes 2048 | tf_op jit(solution)/shard_map/slice | solution.py:330
  132.8 1.1 copy-start.2
  137.6 14.9 %copy-start.3 = (bf16[2,3072,1,128]{3,1,2,0:T(8,128)(2,1)S(1)}, bf16[2,3072,1,128]{3,1,2,0:T(8,128)(2,1)}, u32[]{:S(2)}) copy-start(bf16[2,3072,1,128]{3,1,2,0:T(8,128)(2,1)} %param.26) | copy-start | bytes 4718596
  137.6 55.5 %all-to-all-start.2 = ((bf16[8,72,256]{2,1,0:T(8,128)(2,1)}), bf16[8,72,256]{2,1,0:T(8,128)(2,1)S(1)}, u32[]{:S(2)}, u32[]{:S(2)}) async-start(bf16[8,72,256]{2,1,0:T(8,128)(2,1)} %fresh.1), calls=%async_computation.2 | async-start | bytes 589824 | tf_op jit(solution)/shard_map/all_to_all | solution.py:331
